TPU v7x, 32 devices: a whole 2x2x4 slice. The times are simulated.
32 devices in a mesh: sp: 8 (over z, y), tp: 4 (over x, core).
Axes of the slice: x: 2, y: 2, z: 4, core: 2. Of those that a mesh axis runs over, the one named last changes fastest.
Arguments:
- query_proj: bfloat16 [8192, 2048], P('sp', 'tp'), may hold values from -6 to 6
- key_proj: bfloat16 [8192, 2048], P('sp', 'tp'), may hold values from -6 to 6
- value_proj: bfloat16 [8192, 4096], P('sp', 'tp'), may hold values from -6 to 6
- gate_proj: bfloat16 [8192, 4096], P('sp', 'tp'), may hold values from -6 to 6
- log_decay: float32 [8192, 8], P('sp', 'tp'), may hold values from -0.75 to 0, as said below
- residual: bfloat16 [8192, 2048], P('sp'), may hold values from -4 to 4
- out_weight: bfloat16 [4096, 2048], P('tp'), may hold values from -0.09375 to 0.09375
- norm_gain: float32 [2, 2048], replicated, may hold values from 0.1 to 1.9
- norm_bias: float32 [2, 2048], replicated, may hold values from -1.5 to 1.5
- up_gate: bfloat16 [2048, 5632], P('sp', 'tp'), may hold values from -0.125 to 0.125
- up_value: bfloat16 [2048, 5632], P('sp', 'tp'), may hold values from -0.125 to 0.125
- conv_weight: float32 [2, 3, 5632], P(None, None, 'tp'), may hold values from -3 to 3
- conv_bias: float32 [2, 5632], P(None, 'tp'), may hold values from -1.5 to 1.5
- down_weight: bfloat16 [5632, 2048], P('tp', 'sp'), may hold values from -0.078125 to 0.078125
Outputs:
- layer_output: bfloat16 [8192, 2048], P(('sp', 'tp'))
Inputs may be any that keep to these rules, and one draw needn't show every extreme that they name: `log_decay`: all entries are negative.
All inputs are finite; a program needn't handle non-finite values.
Results may differ from a plain program's by a relative error of at most 0.023.
Values may be sent and summed in bfloat16 or wider, within the bound.
A program may use at most 128 MiB of HBM per device.

v0:
```python
import numpy as np
import jax
import jax.numpy as jnp
from jax import lax
from jax.experimental import pallas as pl
from jax.experimental.pallas import tpu as pltpu
from jax.sharding import PartitionSpec as P

BLOCK = 256
HALO = 16
ROW_CHUNKS = 4

alpha_scale = 8.0**0.25
rope_base = 10000.0
tiny_stabilizer = 1e-05
MESH = pl.DeviceIdType.MESH
F32, BF16 = jnp.float32, jnp.bfloat16


def dot(a, b):
    return jnp.dot(a, b, preferred_element_type=F32)


def dot_t(a, b, dims, precision=None):
    return lax.dot_general(a, b, (dims, ((), ())), precision=precision, preferred_element_type=F32)


def layout(sp, tp):
    cores = 2 if tp % 2 == 0 else 1
    lines = tp // cores
    ny = lines if sp % lines == 0 else 1
    return cores, lines, ny, sp // ny


def rotary_tables(head_width, blocks):
    half = head_width // 2
    freq = rope_base ** (-2.0 * np.arange(half, dtype=np.float64) / head_width)
    inner = np.arange(BLOCK, dtype=np.float64)[:, None] * freq
    outer = (np.arange(blocks, dtype=np.float64) * BLOCK)[:, None] * freq
    tables = (np.cos(inner), np.sin(inner), np.cos(outer), np.sin(outer))
    return [jnp.asarray(t.astype(np.float32)) for t in tables]


class Sends:
    def __init__(self):
        self.left = []

    def start(self, copy, cond=None):
        self.left.append((copy, cond))
        if cond is None:
            copy.start()
        else:
            pl.when(cond)(copy.start)

    def drain(self):
        for copy, cond in self.left:
            if cond is None:
                copy.wait_send()
            else:
                pl.when(cond)(copy.wait_send)
        self.left = []


def make_kernel(n_sp, n_tp, tok_rows, heads, key_width, value_width, width, depth, hidden):
    cores, lines, ny, nz = layout(n_sp, n_tp)
    nb = tok_rows // BLOCK
    own = tok_rows // n_tp
    piece = width // n_sp
    slice_w = value_width // ny
    half_k = key_width // 2
    dh, hh = depth // 2, hidden // 2
    chunk = own // ROW_CHUNKS
    hcols = 128 if hidden % 128 == 0 else hidden

    def kernel(
        cos_in, sin_in, cos_out, sin_out, log_ref, gain, bias, taps, shift,
        q_hbm, k_hbm, v_hbm, g_hbm, res_hbm, ow_hbm, upg, upv, down,
        out,
        wg, wd, qb, kb, vb, gb, ow, res, cum_col, st, lb, within,
        xs, xr, dec, chain_s, chain_r, cb, cs, part, r1, s2, r2, acc, rows, ups, act,
        load_sem, bulk_r, bulk_z, bulk_y, st_s, st_r, dec_s, dec_r, ch_s, ch_r, cb_s, cb_r,
        rs1_s, rs1_r, rs2_s, rs2_r, ag_s, ag_r, agf_s, halo_s, halo_r,
    ):
        sp, tp = lax.axis_index("sp"), lax.axis_index("tp")
        z, y = sp // ny, sp % ny
        x, c = tp // cores, tp % cores
        me_sp = sp

        def remote(src, dst, ssem, rsem, to_sp, to_tp):
            return pltpu.make_async_remote_copy(
                src_ref=src, dst_ref=dst, send_sem=ssem, recv_sem=rsem,
                device_id=(to_sp, to_tp), device_id_type=MESH,
            )

        def arrived(dst, ssem, rsem, cond=None):
            copy = remote(dst, dst, ssem, rsem, sp, tp)
            if cond is None:
                copy.wait_recv()
            else:
                pl.when(cond)(copy.wait_recv)

        own_rows = pl.ds(pl.multiple_of(tp * own, own), own)
        pairs = [
            (k_hbm, kb), (v_hbm, vb), (q_hbm, qb), (g_hbm, gb), (ow_hbm, ow),
            (res_hbm.at[own_rows], res), (upg, wg.at[me_sp, 0]), (upv, wg.at[me_sp, 1]),
            (down, wd.at[me_sp]),
        ]
        loads = [pltpu.make_async_copy(a, b, load_sem.at[i]) for i, (a, b) in enumerate(pairs)]
        for load in loads:
            load.start()

        barrier = pltpu.get_barrier_semaphore()

        def greet(to_sp, to_tp, cond=None):
            def go():
                pl.semaphore_signal(barrier, inc=1, device_id=(to_sp, to_tp), device_id_type=MESH)

            if cond is None:
                go()
            else:
                pl.when(cond)(go)

        other_y = [z * ny + (y + d) % ny for d in range(1, ny)]
        other_c = [x * cores + (c + d) % cores for d in range(1, cores)]
        other_x = [(x + d) % lines * cores + c for d in range(1, lines)]
        peers = [(sp + ny, tp, z < nz - 1), (sp - ny, tp, z > 0)]
        peers += [(o, tp, None) for o in other_y]
        peers += [(sp, o, None) for o in other_c + other_x]
        for t in range(n_tp):
            peers.append((sp + 1, t, jnp.logical_and(tp == n_tp - 1, sp < n_sp - 1)))
        for to_sp, to_tp, cond in peers:
            greet(to_sp, to_tp, cond)
        greet(sp - 1, n_tp - 1, sp > 0)
        count = (sp > 0).astype(jnp.int32)
        for _, _, cond in peers:
            count = count + (1 if cond is None else cond.astype(jnp.int32))
        pl.semaphore_wait(barrier, count)

        bulk = Sends()

        def slot(p, src):
            m, h = p // 2, p % 2
            if m < 2:
                return wg.at[src, m, pl.ds(h * dh, dh)]
            return wd.at[src, pl.ds(h * hh, hh)]

        def mine(p):
            m, h = p // 2, p % 2
            if m == 2:
                return down.at[pl.ds(h * hh, hh)]
            return (upg, upv)[m].at[pl.ds(h * dh, dh)]

        def own_z(p, up):
            cond, to = (z < nz - 1, sp + ny) if up else (z > 0, sp - ny)
            bulk.start(
                remote(mine(p), slot(p, sp), bulk_z.at[p, 0 if up else 1], bulk_r.at[p, sp], to, tp),
                cond,
            )

        def own_y(p):
            for d, to in enumerate(other_y):
                bulk.start(
                    remote(mine(p), slot(p, sp), bulk_y.at[p, 0, d], bulk_r.at[p, sp], to, tp)
                )

        def source(up, d):
            return (sp - d * ny, z >= d) if up else (sp + d * ny, z < nz - d)

        def take(p, up, d):
            src, cond = source(up, d)
            src = jnp.clip(src, 0, n_sp - 1)
            arrived(slot(p, src), bulk_z.at[p, 0], bulk_r.at[p, src], cond)

        def on_z(p, up, d):
            src, cond = source(up, d)
            src = jnp.clip(src, 0, n_sp - 1)
            to, more = (sp + ny, z < nz - 1) if up else (sp - ny, z > 0)
            sem = bulk_z.at[p, 2 * d + (0 if up else 1)]
            bulk.start(
                remote(slot(p, src), slot(p, src), sem, bulk_r.at[p, src], to, tp),
                jnp.logical_and(cond, more),
            )

        def on_y(p, up, d):
            src, cond = source(up, d)
            src = jnp.clip(src, 0, n_sp - 1)
            for e, to in enumerate(other_y):
                sem = bulk_y.at[p, 2 * d + (0 if up else 1), e]
                bulk.start(
                    remote(slot(p, src), slot(p, src), sem, bulk_r.at[p, src], to, tp), cond
                )

        def relay(m, up, d):
            if d >= nz:
                return
            for p in (2 * m, 2 * m + 1):
                take(p, up, d)
                if d < nz - 1:
                    on_z(p, up, d)
                on_y(p, up, d)

        def side_arrivals(m):
            for src in range(n_sp):
                for p in (2 * m, 2 * m + 1):
                    arrived(slot(p, src), bulk_z.at[p, 0], bulk_r.at[p, src], src % ny != y)

        for p in (0, 1):
            own_z(p, True)
        for p in (0, 1, 2, 3):
            own_z(p, False)
        own_y(0)

        ii = lax.broadcasted_iota(jnp.int32, (BLOCK, BLOCK), 0)
        jj = lax.broadcasted_iota(jnp.int32, (BLOCK, BLOCK), 1)
        lower = (ii >= jj).astype(F32)
        logs = log_ref[...]
        cum_col[...] = dot_t(lower, logs, ((1,), (1,)), lax.Precision.HIGHEST)

        def column(idx):
            lane = lax.broadcasted_iota(jnp.int32, cum_col.shape, 1)
            return jnp.sum(jnp.where(lane == idx, cum_col[...], 0.0), axis=1, keepdims=True)

        def angles(b):
            row = pl.ds(sp * nb + b, 1)
            co, so = cos_out[row, :], sin_out[row, :]
            ci, si = cos_in[...], sin_in[...]
            return ci * co - si * so, si * co + ci * so

        def rotated(value, cosine, sine):
            front, second = value[:, :half_k], value[:, half_k:]
            return jnp.concatenate(
                [front * cosine - second * sine, front * sine + second * cosine], axis=1
            )

        def block_rows(b):
            return pl.ds(pl.multiple_of(b * BLOCK, BLOCK), BLOCK)

        loads[0].wait()
        loads[1].wait()
        st[...] = jnp.zeros_like(st)

        def local_states(b, _):
            r = block_rows(b)
            cosine, sine = angles(b)
            for h in range(heads):
                cc = column(h * nb + b)
                total = cc[BLOCK - 1 : BLOCK, :]
                kc = pl.ds(h * key_width, key_width)
                key = rotated(kb[r, kc].astype(F32), cosine, sine) * key_width ** (-0.5)
                key = key.astype(BF16)
                kb[r, kc] = key
                faded = (key.astype(F32) * jnp.exp(total - cc)).astype(BF16)
                term = dot_t(faded, vb[r, pl.ds(h * value_width, value_width)], ((0,), (0,)))
                before = st[h]
                lb[b * heads + h] = before.astype(BF16)
                st[h] = jnp.exp(total) * before + term
            return 0

        lax.fori_loop(0, nb, local_states, 0)

        def head_log(h):
            total = jnp.zeros((1, 1), F32)
            for b in range(nb):
                total = total + jnp.sum(logs[h * nb + b : h * nb + b + 1, :], axis=1, keepdims=True)
            return total

        hrow = lax.broadcasted_iota(jnp.int32, (8, 128), 0)
        tile = jnp.zeros((8, 128), F32)
        for h in range(heads):
            tile = jnp.where(hrow == h, head_log(h), tile)
        dec[pl.ds(y, 1)] = tile[None]
        states = Sends()
        for d, to in enumerate(other_y):
            far = (y + d + 1) % ny
            states.start(
                remote(dec.at[y], dec.at[y], dec_s.at[d], dec_r.at[y], to, tp)
            )
            for h in range(heads):
                for f in range(ny):

                    @pl.when(far == f)
                    def _():
                        xs[d, h] = st[h, :, f * slice_w : (f + 1) * slice_w].astype(BF16)

                states.start(
                    remote(xs.at[d, h], xr.at[y, h], st_s.at[d, h], st_r.at[y, h], to, tp)
                )
        for p in (1, 2, 3):
            own_y(p)

        loads[2].wait()

        def within_block(b, _):
            r = block_rows(b)
            cosine, sine = angles(b)
            for h in range(heads):
                cc = column(h * nb + b)
                kc = pl.ds(h * key_width, key_width)
                query = rotated(qb[r, kc].astype(F32), cosine, sine).astype(BF16)
                scores = dot_t(query, kb[r, kc], ((1,), (1,)))
                crow = jnp.sum(jnp.where(ii == jj, cc, 0.0), axis=0, keepdims=True)
                gap = jnp.where(ii >= jj, cc - crow, 0.0)
                weight = jnp.where(ii >= jj, jnp.exp(gap), 0.0)
                vc = pl.ds(h * value_width, value_width)
                within[r, vc] = dot((scores * weight).astype(BF16), vb[r, vc])
                qb[r, kc] = (query.astype(F32) * jnp.exp(cc)).astype(BF16)
            return 0

        lax.fori_loop(0, nb, within_block, 0)

        for p in (0, 1):
            take(p, False, 1)
            if nz > 2:
                on_z(p, False, 1)

        for f in range(ny):

            @pl.when(y == f)
            def _():
                for h in range(heads):
                    xr[f, h] = st[h, :, f * slice_w : (f + 1) * slice_w].astype(BF16)

        for d in range(1, ny):
            src = (y + d) % ny
            arrived(dec.at[src], dec_s.at[0], dec_r.at[src])
            for h in range(heads):
                arrived(xr.at[src, h], st_s.at[0, 0], st_r.at[src, h])
        for h in range(heads):

            @pl.when(z == 0)
            def _():
                chain_r[h] = jnp.zeros((key_width, slice_w), BF16)

            arrived(chain_r.at[h], ch_s.at[h], ch_r.at[h], z > 0)
            incoming = chain_r[h].astype(F32)
            before = incoming
            for f in range(ny):
                cb_mine = before.astype(BF16)

                @pl.when(y == f)
                def _():
                    cb[y, h] = cb_mine

                @pl.when(y != f)
                def _():
                    cs[f, h] = cb_mine

                decay = jnp.exp(dec[f, h : h + 1, 0:1])
                before = decay * before + xr[f, h].astype(F32)
            chain_s[h] = before.astype(BF16)
            states.start(
                remote(chain_s.at[h], chain_r.at[h], ch_s.at[h], ch_r.at[h], sp + ny, tp),
                z < nz - 1,
            )
            for d, to in enumerate(other_y):
                far = (y + d + 1) % ny
                states.start(
                    remote(cs.at[far, h], cb.at[y, h], cb_s.at[d, h], cb_r.at[y, h], to, tp)
                )

        for p in (2, 3):
            own_z(p, True)
        for p in (0, 1):
            on_y(p, False, 1)
            take(p, True, 1)
            if nz > 2:
                on_z(p, True, 1)
            on_y(p, True, 1)

        loads[3].wait()
        for h in range(heads):
            for d in range(1, ny):
                src = (y + d) % ny
                arrived(cb.at[src, h], cb_s.at[0, 0], cb_r.at[src, h])

            def finish(b, decay):
                r = block_rows(b)
                vc = pl.ds(h * value_width, value_width)
                state = jnp.concatenate([cb[f, h].astype(F32) for f in range(ny)], axis=1)
                state = (decay * state + lb[b * heads + h].astype(F32)).astype(BF16)
                mixed = within[r, vc] + dot(qb[r, pl.ds(h * key_width, key_width)], state)
                average = jnp.mean(mixed, axis=1, keepdims=True)
                mixed = mixed - average
                spread = jnp.mean(mixed * mixed, axis=1, keepdims=True)
                gate = gb[r, vc].astype(F32)
                gated = gate * jax.nn.sigmoid(gate) * (mixed * lax.rsqrt(spread + tiny_stabilizer))
                gb[r, vc] = gated.astype(BF16)
                return decay * jnp.exp(column(h * nb + b)[BLOCK - 1 : BLOCK, :])

            lax.fori_loop(0, nb, finish, jnp.ones((1, 1), F32))
        states.drain()

        def owner_rows(xx, cc):
            return pl.ds(pl.multiple_of((xx * cores + cc) * own, own), own)

        def piece_cols(s):
            return pl.ds(pl.multiple_of(s * piece, piece), piece)

        def d2d_copies(s):
            return [
                remote(
                    part.at[s, owner_rows(xx, (c + d) % cores)], r1.at[s, d - 1, xx],
                    rs1_s.at[s, d - 1, xx], rs1_r.at[s, d - 1, xx],
                    sp, x * cores + (c + d) % cores,
                )
                for d in range(1, cores)
                for xx in range(lines)
            ]

        def x_copies(s):
            return [
                remote(
                    s2.at[s, d - 1], r2.at[s, d - 1], rs2_s.at[s, d - 1], rs2_r.at[s, d - 1],
                    sp, (x + d) % lines * cores + c,
                )
                for d in range(1, lines)
            ]

        row_tile = min(tok_rows, 512)

        def product(s, lhs, rhs):
            def one(i, _):
                r = pl.ds(pl.multiple_of(i * row_tile, row_tile), row_tile)
                part[s, r, :] = dot(lhs[r, :], rhs()).astype(BF16)
                return 0

            lax.fori_loop(0, tok_rows // row_tile, one, 0)
            for copy in d2d_copies(s):
                copy.start()

        def combine(s):
            for copy in d2d_copies(s):
                copy.wait_recv()
            for d in range(lines):
                xx = (x + d) % lines
                total = part[s, owner_rows(xx, c), :].astype(F32)
                for e in range(cores - 1):
                    total = total + r1[s, e, xx].astype(F32)
                if d == 0:
                    acc[:, piece_cols(s)] = total
                else:
                    s2[s, d - 1] = total.astype(BF16)
            for copy in x_copies(s):
                copy.start()

        def collect(s):
            for copy in x_copies(s):
                copy.wait_recv()
            total = acc[:, piece_cols(s)]
            for d in range(lines - 1):
                total = total + r2[s, d].astype(F32)
            acc[:, piece_cols(s)] = total

        def release(s, _):
            for copy in d2d_copies(s) + x_copies(s):
                copy.wait_send()
            return 0

        def out_step(s, _):
            product(s, gb, lambda: ow[:, piece_cols(s)])
            pl.when(s > 0)(lambda: combine(s - 1))
            return 0

        loads[4].wait()
        mid = n_sp // 2
        lax.fori_loop(0, mid, out_step, 0)
        relay(1, False, 1)
        lax.fori_loop(mid, n_sp, out_step, 0)
        combine(n_sp - 1)
        relay(0, False, 2)
        relay(1, True, 1)

        def collect_step(s, _):
            collect(s)
            return 0

        lax.fori_loop(0, n_sp, collect_step, 0)
        relay(0, True, 2)

        loads[5].wait()

        def layer_norm(values, which):
            average = jnp.mean(values, axis=1, keepdims=True)
            values = values - average
            spread = jnp.mean(values * values, axis=1, keepdims=True)
            values = values * lax.rsqrt(spread + tiny_stabilizer)
            return values * gain[which : which + 1, :] + bias[which : which + 1, :]

        ln_rows = 16
        gathered = Sends()

        def chunk_of(owner, j):
            return rows.at[pl.ds(pl.multiple_of(HALO + owner * own + j * chunk, 16), chunk)]

        pl.when(sp == 0)(lambda: rows.__setitem__((pl.ds(0, HALO), slice(None)), jnp.zeros((HALO, width), BF16)))
        for j in range(ROW_CHUNKS):

            def norm_rows(i, _):
                at = pl.multiple_of(j * chunk + i * ln_rows, ln_rows)
                r = pl.ds(at, ln_rows)
                value = layer_norm(alpha_scale * res[r, :].astype(F32) + acc[r, :], 0).astype(BF16)
                res[r, :] = value
                rows[pl.ds(pl.multiple_of(HALO + tp * own + at, 16), ln_rows), :] = value
                return 0

            lax.fori_loop(0, chunk // ln_rows, norm_rows, 0)
            for d, to in enumerate(other_c + other_x):
                gathered.start(
                    remote(chunk_of(tp, j), chunk_of(tp, j), ag_s.at[j, d], ag_r.at[j, tp], sp, to)
                )
        last = pl.ds(tok_rows, HALO)
        for t in range(n_tp):
            gathered.start(
                remote(rows.at[last], rows.at[pl.ds(0, HALO)], halo_s.at[t], halo_r, sp + 1, t),
                jnp.logical_and(tp == n_tp - 1, sp < n_sp - 1),
            )
        relay(0, False, 3)
        for j in range(ROW_CHUNKS):
            for d in range(1, lines):
                owner = (x + d) % lines * cores + c
                arrived(chunk_of(owner, j), ag_s.at[j, 0], ag_r.at[j, owner])
                for e, to in enumerate(other_c):
                    gathered.start(
                        remote(
                            chunk_of(owner, j), chunk_of(owner, j),
                            agf_s.at[j, d - 1, e], ag_r.at[j, owner], sp, to,
                        )
                    )
            if j == 1:
                relay(1, False, 2)
                relay(0, True, 3)
        for d in range(1, cores):
            for e in range(lines):
                owner = (x + e) % lines * cores + (c + d) % cores
                for j in range(ROW_CHUNKS):
                    arrived(chunk_of(owner, j), ag_s.at[j, 0], ag_r.at[j, owner])
        relay(1, True, 2)
        relay(1, False, 3)
        for p in (4, 5):
            own_z(p, True)
            own_z(p, False)
        lax.fori_loop(0, n_sp, release, 0)

        def up_tile(m, start, count):
            r = pl.ds(start, count)
            total = None
            for s in range(n_sp):
                term = dot(rows[r, s * depth : (s + 1) * depth], wg[s, m])
                total = term if total is None else total + term
            ups[m, r, :] = total.astype(BF16)

        def up_rows(m):
            def one(i, _):
                up_tile(m, pl.multiple_of(HALO + i * BLOCK, 16), BLOCK)
                return 0

            lax.fori_loop(0, tok_rows // BLOCK, one, 0)
            up_tile(m, 0, HALO)

        loads[6].wait()
        side_arrivals(0)
        arrived(rows.at[pl.ds(0, HALO)], halo_s.at[0], halo_r, sp > 0)
        up_rows(0)
        relay(1, True, 3)
        for p in (4, 5):
            own_y(p)
        loads[7].wait()
        side_arrivals(1)
        up_rows(1)

        def activate(i, col):
            at = pl.multiple_of(i * BLOCK, BLOCK)
            convs = []
            for m in range(2):
                tile = ups[m, pl.ds(at, BLOCK + HALO), col].astype(F32)
                value = shift[m : m + 1, col]
                for j in range(3):
                    value = value + taps[m, j : j + 1, col] * tile[HALO - 2 + j : HALO - 2 + j + BLOCK, :]
                convs.append(value)
            act[pl.ds(at, BLOCK), col] = (jax.nn.gelu(convs[0]) * convs[1]).astype(BF16)

        def activate_step(i, _):
            for t in range(hidden // hcols):
                activate(i, pl.ds(t * hcols, hcols))
            return 0

        lax.fori_loop(0, tok_rows // BLOCK, activate_step, 0)

        order = [
            [zz] + sorted((o for o in range(nz) if o != zz), key=lambda o: (abs(o - zz), abs(2 * o - nz + 1)))
            for zz in range(nz)
        ]

        def nearest(k):
            got = jnp.int32(order[0][k])
            for zz in range(1, nz):
                got = jnp.where(z == zz, order[zz][k], got)
            return got

        steps = [(k, 0) for k in range(nz)] + [(k, d) for k in range(nz) for d in range(1, ny)]
        loads[8].wait()
        previous = None
        done = []
        for k, d in steps:
            src_z = nearest(k)
            src = src_z * ny + (y + d) % ny
            if d > 0 or k > 0:
                for p in (4, 5):
                    arrived(slot(p, src), bulk_z.at[p, 0], bulk_r.at[p, src])
            if d == 0 and k > 0:
                to_z = jnp.where(src_z < z, z + 1, z - 1)
                more = jnp.logical_and(to_z >= 0, to_z < nz)
                for p in (4, 5):
                    bulk.start(
                        remote(slot(p, src), slot(p, src), bulk_z.at[p, 1 + k], bulk_r.at[p, src], to_z * ny + y, tp),
                        more,
                    )
                    for e, to in enumerate(other_y):
                        bulk.start(
                            remote(slot(p, src), slot(p, src), bulk_y.at[p, k, e], bulk_r.at[p, src], to, tp)
                        )
            product(src, act, lambda: wd[src])
            if previous is not None:
                combine(previous)
            previous = src
            done.append(src)
        combine(previous)
        for src in done:
            collect(src)

        def final_rows(i, _):
            r = pl.ds(pl.multiple_of(i * ln_rows, ln_rows), ln_rows)
            out[r, :] = layer_norm(alpha_scale * res[r, :].astype(F32) + acc[r, :], 1).astype(BF16)
            return 0

        lax.fori_loop(0, own // ln_rows, final_rows, 0)
        lax.fori_loop(0, n_sp, release, 0)
        gathered.drain()
        bulk.drain()

    vmem, dma = pltpu.VMEM, pltpu.SemaphoreType.DMA
    oc, ol, oy = max(cores - 1, 1), max(lines - 1, 1), max(ny - 1, 1)
    scratch = [
        vmem((n_sp, 2, depth, hidden), BF16),
        vmem((n_sp, hidden, piece), BF16),
        vmem((tok_rows, heads * key_width), BF16),
        vmem((tok_rows, heads * key_width), BF16),
        vmem((tok_rows, heads * value_width), BF16),
        vmem((tok_rows, heads * value_width), BF16),
        vmem((heads * value_width, width), BF16),
        vmem((own, width), BF16),
        vmem((BLOCK, heads * nb), F32),
        vmem((heads, key_width, value_width), F32),
        vmem((nb * heads, key_width, value_width), BF16),
        vmem((tok_rows, heads * value_width), F32),
        vmem((oy, heads, key_width, slice_w), BF16),
        vmem((ny, heads, key_width, slice_w), BF16),
        vmem((ny, 8, 128), F32),
        vmem((heads, key_width, slice_w), BF16),
        vmem((heads, key_width, slice_w), BF16),
        vmem((ny, heads, key_width, slice_w), BF16),
        vmem((ny, heads, key_width, slice_w), BF16),
        vmem((n_sp, tok_rows, piece), BF16),
        vmem((n_sp, oc, lines, own, piece), BF16),
        vmem((n_sp, ol, own, piece), BF16),
        vmem((n_sp, ol, own, piece), BF16),
        vmem((own, width), F32),
        vmem((HALO + tok_rows, width), BF16),
        vmem((2, HALO + tok_rows, hidden), BF16),
        vmem((tok_rows, hidden), BF16),
        dma((9,)),
        dma((6, n_sp)),
        dma((6, 2 * nz)),
        dma((6, 2 * nz, oy)),
        dma((oy, heads)),
        dma((ny, heads)),
        dma((oy,)),
        dma((ny,)),
        dma((heads,)),
        dma((heads,)),
        dma((oy, heads)),
        dma((ny, heads)),
        dma((n_sp, oc, lines)),
        dma((n_sp, oc, lines)),
        dma((n_sp, ol)),
        dma((n_sp, ol)),
        dma((ROW_CHUNKS, cores + lines)),
        dma((ROW_CHUNKS, n_tp)),
        dma((ROW_CHUNKS, ol, oc)),
        dma((n_tp,)),
        dma(()),
    ]
    in_specs = [pl.BlockSpec(memory_space=pltpu.VMEM)] * 9 + [pl.BlockSpec(memory_space=pl.ANY)] * 9
    return pl.pallas_call(
        kernel,
        out_shape=jax.ShapeDtypeStruct((own, width), BF16),
        in_specs=in_specs,
        out_specs=pl.BlockSpec(memory_space=pltpu.VMEM),
        scratch_shapes=scratch,
        compiler_params=pltpu.CompilerParams(
            collective_id=0, has_side_effects=True, vmem_limit_bytes=67_000_000
        ),
    )


def shards(
    query_proj, key_proj, value_proj, gate_proj, log_decay, residual, out_weight, norm_gain,
    norm_bias, up_gate, up_value, conv_weight, conv_bias, down_weight,
):
    n_sp, n_tp = lax.axis_size("sp"), lax.axis_size("tp")
    tok_rows, heads = log_decay.shape
    key_width = query_proj.shape[1] // heads
    value_width = value_proj.shape[1] // heads
    nb = tok_rows // BLOCK
    call = make_kernel(
        n_sp, n_tp, tok_rows, heads, key_width, value_width,
        residual.shape[1], up_gate.shape[0], up_gate.shape[1],
    )
    tables = rotary_tables(key_width, n_sp * nb)
    logs = log_decay.T.reshape(heads * nb, BLOCK)
    return call(
        *tables, logs, norm_gain, norm_bias, conv_weight, conv_bias, query_proj, key_proj,
        value_proj, gate_proj, residual, out_weight, up_gate, up_value, down_weight,
    )


def solution(mesh):
    placed = (
        P("sp", "tp"), P("sp", "tp"), P("sp", "tp"), P("sp", "tp"), P("sp", "tp"),
        P("sp", None), P("tp", None), P(), P(), P("sp", "tp"), P("sp", "tp"),
        P(None, None, "tp"), P(None, "tp"), P("tp", "sp"),
    )
    return jax.shard_map(
        shards, mesh=mesh, in_specs=placed, out_specs=P(("sp", "tp"), None), check_vma=False
    )
```

profile of v0, /device:TPU:30, one launch (start us, length us, event | category | flops | bytes accessed | tf_op | source)
XLA Modules:
  0.0 229.1 jit_solution(11126938887440478718)
XLA Ops:
  0.0 1.3 reshape.3.log_ref
  1.3 1.4 copy.19.taps
  2.7 224.1 %shard_map.172 = bf16[256,2048]{1,0:T(8,128)(2,1)} custom-call(f32[256,128]{1,0:T(8,128)} %constant.8.clone.cos_in, f32[256,128]{1,0:T(8,128)} %constant.9.clone.sin_in, f32[32,128]{1,0:T(8,128)} %constant.10.clone.cos_out, f32[32,128]{1,0:T(8,128)} %constant.11.clone.sin_out, f32[8,256]{1,0:T(8,128)} %reshape.3.log_ref, f32[2,2048]{1,0:T(2,128)} %gain.1, ...), custom_call_target="tpu_custom_call" | custom-call | tf_op jit(solution)/shard_map/pallas_call | solution.py:721
  226.8 2.3 %copy.21 = bf16[256,2048]{1,0:T(8,128)(2,1)} copy(bf16[256,2048]{1,0:T(8,128)(2,1)} %shard_map.172) | data formatting | bytes 2097152
where the time goes:
time: 234 us; the launch traced here: 229 us
  Pallas kernels  224 us (96%)
  local copies, waits for them, and re-layouts  4.99 us (2%)
    pallas_call x1, Pallas kernels, shards(): call(*tables, logs, norm_gain, norm_bias, conv_weight, conv_bias, query_p...  224 us

commit v1 on v0

--- a/solution.py
+++ b/solution.py
@@ -150,8 +150,10 @@
                 return down.at[pl.ds(h * hh, hh)]
             return (upg, upv)[m].at[pl.ds(h * dh, dh)]
 
-        def own_z(p, up):
+        def own_z(p, up, also=None):
             cond, to = (z < nz - 1, sp + ny) if up else (z > 0, sp - ny)
+            if also is not None:
+                cond = jnp.logical_and(cond, also)
             bulk.start(
                 remote(mine(p), slot(p, sp), bulk_z.at[p, 0 if up else 1], bulk_r.at[p, sp], to, tp),
                 cond,
@@ -163,16 +165,19 @@
                     remote(mine(p), slot(p, sp), bulk_y.at[p, 0, d], bulk_r.at[p, sp], to, tp)
                 )
 
-        def source(up, d):
-            return (sp - d * ny, z >= d) if up else (sp + d * ny, z < nz - d)
-
-        def take(p, up, d):
-            src, cond = source(up, d)
+        middle = jnp.logical_and(z > 0, z < nz - 1)
+
+        def source(up, d, also=None):
+            src, cond = (sp - d * ny, z >= d) if up else (sp + d * ny, z < nz - d)
+            return src, cond if also is None else jnp.logical_and(cond, also)
+
+        def take(p, up, d, also=None):
+            src, cond = source(up, d, also)
             src = jnp.clip(src, 0, n_sp - 1)
             arrived(slot(p, src), bulk_z.at[p, 0], bulk_r.at[p, src], cond)
 
-        def on_z(p, up, d):
-            src, cond = source(up, d)
+        def on_z(p, up, d, also=None):
+            src, cond = source(up, d, also)
             src = jnp.clip(src, 0, n_sp - 1)
             to, more = (sp + ny, z < nz - 1) if up else (sp - ny, z > 0)
             sem = bulk_z.at[p, 2 * d + (0 if up else 1)]
@@ -181,8 +186,46 @@
                 jnp.logical_and(cond, more),
             )
 
-        def on_y(p, up, d):
-            src, cond = source(up, d)
+        balanced = ny == 2 and nz >= 4
+
+        def by_y(p, src_z):
+            if not balanced:
+                return jnp.bool_(True)
+            m, h = p // 2, p % 2
+            skip = jnp.logical_or(
+                jnp.logical_and(z == 1, src_z == 0),
+                jnp.logical_and(z == nz - 2, src_z == nz - 1),
+            )
+            if m == 2 or h == 1:
+                skip = jnp.logical_or(skip, jnp.logical_and(z == 0, src_z == 1))
+            if h == 1:
+                skip = jnp.logical_or(skip, jnp.logical_and(z == nz - 1, src_z == nz - 2))
+            return jnp.logical_not(skip)
+
+        def beside(p):
+            m, h = p // 2, p % 2
+            src = z * ny + (y + 1) % ny
+            arrived(slot(p, src), bulk_z.at[p, 0], bulk_r.at[p, src])
+            cond = jnp.logical_or(z == 0, z == nz - 1)
+            if h == 1:
+                cond = jnp.logical_or(cond, jnp.logical_or(z == 1, z == nz - 2))
+            elif m == 2:
+                cond = jnp.logical_or(cond, z == 1)
+            down_to = jnp.logical_or(z == 1, z == nz - 1)
+            to = jnp.where(down_to, z - 1, z + 1) * ny + y
+            bulk.start(
+                remote(slot(p, src), slot(p, src), bulk_z.at[p, 2 * nz], bulk_r.at[p, src], to, tp),
+                cond,
+            )
+
+        def share(m):
+            if balanced:
+                beside(2 * m)
+                beside(2 * m + 1)
+
+        def on_y(p, up, d, also=None):
+            src, cond = source(up, d, also)
+            cond = jnp.logical_and(cond, by_y(p, src // ny))
             src = jnp.clip(src, 0, n_sp - 1)
             for e, to in enumerate(other_y):
                 sem = bulk_y.at[p, 2 * d + (0 if up else 1), e]
@@ -190,25 +233,27 @@
                     remote(slot(p, src), slot(p, src), sem, bulk_r.at[p, src], to, tp), cond
                 )
 
-        def relay(m, up, d):
+        def relay(m, up, d, also=None):
             if d >= nz:
                 return
             for p in (2 * m, 2 * m + 1):
-                take(p, up, d)
+                take(p, up, d, also)
                 if d < nz - 1:
-                    on_z(p, up, d)
-                on_y(p, up, d)
+                    on_z(p, up, d, also)
+                on_y(p, up, d, also)
 
         def side_arrivals(m):
             for src in range(n_sp):
                 for p in (2 * m, 2 * m + 1):
-                    arrived(slot(p, src), bulk_z.at[p, 0], bulk_r.at[p, src], src % ny != y)
-
-        for p in (0, 1):
-            own_z(p, True)
+                    cond = src % ny != y
+                    if balanced:
+                        cond = jnp.logical_and(cond, src // ny != z)
+                    arrived(slot(p, src), bulk_z.at[p, 0], bulk_r.at[p, src], cond)
+
+        own_z(0, True)
+        own_z(1, True, z > 0)
         for p in (0, 1, 2, 3):
             own_z(p, False)
-        own_y(0)
 
         ii = lax.broadcasted_iota(jnp.int32, (BLOCK, BLOCK), 0)
         jj = lax.broadcasted_iota(jnp.int32, (BLOCK, BLOCK), 1)
@@ -285,8 +330,8 @@
                 states.start(
                     remote(xs.at[d, h], xr.at[y, h], st_s.at[d, h], st_r.at[y, h], to, tp)
                 )
-        for p in (1, 2, 3):
-            own_y(p)
+        own_y(0)
+        own_y(1)
 
         loads[2].wait()
 
@@ -308,11 +353,6 @@
 
         lax.fori_loop(0, nb, within_block, 0)
 
-        for p in (0, 1):
-            take(p, False, 1)
-            if nz > 2:
-                on_z(p, False, 1)
-
         for f in range(ny):
 
             @pl.when(y == f)
@@ -358,14 +398,12 @@
                     remote(cs.at[far, h], cb.at[y, h], cb_s.at[d, h], cb_r.at[y, h], to, tp)
                 )
 
+        own_z(1, True, z == 0)
         for p in (2, 3):
             own_z(p, True)
-        for p in (0, 1):
-            on_y(p, False, 1)
-            take(p, True, 1)
-            if nz > 2:
-                on_z(p, True, 1)
-            on_y(p, True, 1)
+            own_y(p)
+        relay(0, False, 1)
+        share(0)
 
         loads[3].wait()
         for h in range(heads):
@@ -389,6 +427,7 @@
 
             lax.fori_loop(0, nb, finish, jnp.ones((1, 1), F32))
         states.drain()
+        relay(0, True, 1)
 
         def owner_rows(xx, cc):
             return pl.ds(pl.multiple_of((xx * cores + cc) * own, own), own)
@@ -462,12 +501,11 @@
             return 0
 
         loads[4].wait()
-        mid = n_sp // 2
-        lax.fori_loop(0, mid, out_step, 0)
-        relay(1, False, 1)
-        lax.fori_loop(mid, n_sp, out_step, 0)
+        lax.fori_loop(0, n_sp, out_step, 0)
         combine(n_sp - 1)
         relay(0, False, 2)
+        relay(0, True, 2)
+        relay(1, False, 1)
         relay(1, True, 1)
 
         def collect_step(s, _):
@@ -475,7 +513,6 @@
             return 0
 
         lax.fori_loop(0, n_sp, collect_step, 0)
-        relay(0, True, 2)
 
         loads[5].wait()
 
@@ -486,7 +523,7 @@
             values = values * lax.rsqrt(spread + tiny_stabilizer)
             return values * gain[which : which + 1, :] + bias[which : which + 1, :]
 
-        ln_rows = 16
+        ln_rows = 32
         gathered = Sends()
 
         def chunk_of(owner, j):
@@ -514,8 +551,14 @@
                 remote(rows.at[last], rows.at[pl.ds(0, HALO)], halo_s.at[t], halo_r, sp + 1, t),
                 jnp.logical_and(tp == n_tp - 1, sp < n_sp - 1),
             )
-        relay(0, False, 3)
         for j in range(ROW_CHUNKS):
+            if j == ROW_CHUNKS // 2:
+                relay(0, False, 3)
+                relay(1, False, 2, z > 0)
+                relay(1, True, 2, z < nz - 1)
+                share(1)
+            if j == ROW_CHUNKS - 1:
+                relay(0, True, 3)
             for d in range(1, lines):
                 owner = (x + d) % lines * cores + c
                 arrived(chunk_of(owner, j), ag_s.at[j, 0], ag_r.at[j, owner])
@@ -526,19 +569,19 @@
                             agf_s.at[j, d - 1, e], ag_r.at[j, owner], sp, to,
                         )
                     )
-            if j == 1:
-                relay(1, False, 2)
-                relay(0, True, 3)
         for d in range(1, cores):
             for e in range(lines):
                 owner = (x + e) % lines * cores + (c + d) % cores
                 for j in range(ROW_CHUNKS):
                     arrived(chunk_of(owner, j), ag_s.at[j, 0], ag_r.at[j, owner])
-        relay(1, True, 2)
-        relay(1, False, 3)
         for p in (4, 5):
+            own_z(p, False)
             own_z(p, True)
-            own_z(p, False)
+        relay(1, False, 2, z == 0)
+        relay(1, True, 2, z == nz - 1)
+        for d in range(4, nz):
+            relay(0, False, d)
+            relay(0, True, d)
         lax.fori_loop(0, n_sp, release, 0)
 
         def up_tile(m, start, count):
@@ -561,9 +604,13 @@
         side_arrivals(0)
         arrived(rows.at[pl.ds(0, HALO)], halo_s.at[0], halo_r, sp > 0)
         up_rows(0)
-        relay(1, True, 3)
-        for p in (4, 5):
-            own_y(p)
+        for d in range(3, nz):
+            relay(1, False, d)
+            relay(1, True, d)
+        own_y(4)
+        own_y(5)
+        relay(2, False, 1, middle)
+        relay(2, True, 1, middle)
         loads[7].wait()
         side_arrivals(1)
         up_rows(1)
@@ -597,27 +644,40 @@
                 got = jnp.where(z == zz, order[zz][k], got)
             return got
 
-        steps = [(k, 0) for k in range(nz)] + [(k, d) for k in range(nz) for d in range(1, ny)]
+        first = [(k, 0) for k in range(nz)]
+        second = [(k, d) for k in range(nz) for d in range(1, ny)]
+        steps = first[:-1] + second[: ny - 1] + first[-1:] + second[ny - 1 :]
         loads[8].wait()
         previous = None
         done = []
         for k, d in steps:
             src_z = nearest(k)
             src = src_z * ny + (y + d) % ny
-            if d > 0 or k > 0:
+            if balanced and d > 0 and k == 0:
+                share(2)
+            elif d > 0:
                 for p in (4, 5):
                     arrived(slot(p, src), bulk_z.at[p, 0], bulk_r.at[p, src])
-            if d == 0 and k > 0:
+            elif k > 0:
                 to_z = jnp.where(src_z < z, z + 1, z - 1)
                 more = jnp.logical_and(to_z >= 0, to_z < nz)
+                fresh = jnp.logical_not(jnp.logical_and(middle, jnp.abs(src_z - z) == 1))
                 for p in (4, 5):
+                    arrived(slot(p, src), bulk_z.at[p, 0], bulk_r.at[p, src], fresh)
                     bulk.start(
-                        remote(slot(p, src), slot(p, src), bulk_z.at[p, 1 + k], bulk_r.at[p, src], to_z * ny + y, tp),
-                        more,
+                        remote(
+                            slot(p, src), slot(p, src), bulk_z.at[p, 2 * nz + k],
+                            bulk_r.at[p, src], to_z * ny + y, tp,
+                        ),
+                        jnp.logical_and(more, fresh),
                     )
                     for e, to in enumerate(other_y):
                         bulk.start(
-                            remote(slot(p, src), slot(p, src), bulk_y.at[p, k, e], bulk_r.at[p, src], to, tp)
+                            remote(
+                                slot(p, src), slot(p, src), bulk_y.at[p, 2 * nz + k, e],
+                                bulk_r.at[p, src], to, tp,
+                            ),
+                            jnp.logical_and(by_y(p, src_z), fresh),
                         )
             product(src, act, lambda: wd[src])
             if previous is not None:
@@ -670,8 +730,8 @@
         vmem((tok_rows, hidden), BF16),
         dma((9,)),
         dma((6, n_sp)),
-        dma((6, 2 * nz)),
-        dma((6, 2 * nz, oy)),
+        dma((6, 3 * nz)),
+        dma((6, 3 * nz, oy)),
         dma((oy, heads)),
         dma((ny, heads)),
         dma((oy,)),

time: 234 us -> 211 us (0.902); the launches traced: 229 us -> 211 us
  Pallas kernels: 224 us -> 206 us
    pallas_call x1, Pallas kernels: 224 us -> 206 us  [shards(): call(*tables, logs, norm_gain, norm_bias, conv_weight, conv_bias, query_p...]
where the time goes in v1:
time: 211 us
  Pallas kernels  206 us (98%)
  local copies, waits for them, and re-layouts  4.99 us (2%)
    pallas_call x1, Pallas kernels, shards(): call(*tables, logs, norm_gain, norm_bias, conv_weight, conv_bias, query_p...  206 us

profile of v1, /device:TPU:30, one launch (start us, length us, event | category | flops | bytes accessed | tf_op | source)
XLA Modules:
  0.0 210.5 jit_solution(6880266292399916774)
XLA Ops:
  0.0 1.3 reshape.3.log_ref
  1.3 1.4 copy.19.taps
  2.7 205.5 %shard_map.172 = bf16[256,2048]{1,0:T(8,128)(2,1)} custom-call(f32[256,128]{1,0:T(8,128)} %constant.8.clone.cos_in, f32[256,128]{1,0:T(8,128)} %constant.9.clone.sin_in, f32[32,128]{1,0:T(8,128)} %constant.10.clone.cos_out, f32[32,128]{1,0:T(8,128)} %constant.11.clone.sin_out, f32[8,256]{1,0:T(8,128)} %reshape.3.log_ref, f32[2,2048]{1,0:T(2,128)} %gain.1, ...), custom_call_target="tpu_custom_call" | custom-call | tf_op jit(solution)/shard_map/pallas_call | solution.py:781
  208.2 2.3 %copy.21 = bf16[256,2048]{1,0:T(8,128)(2,1)} copy(bf16[256,2048]{1,0:T(8,128)(2,1)} %shard_map.172) | data formatting | bytes 2097152

commit v2 on v1

--- a/solution.py
+++ b/solution.py
@@ -763,6 +763,817 @@
     )
 
 
+def make_square_kernel(n_sp, n_tp, tok_rows, heads, key_width, value_width, width, depth, hidden):
+    cores, lines, ny, nz = layout(n_sp, n_tp)
+    nb = tok_rows // BLOCK
+    own = tok_rows // n_tp
+    piece = width // n_sp
+    slice_w = value_width // ny
+    half_k = key_width // 2
+    dh, hh = depth // 2, hidden // 2
+    chunk = own // ROW_CHUNKS
+    hcols = 128 if hidden % 128 == 0 else hidden
+
+    def kernel(
+        cos_in, sin_in, cos_out, sin_out, log_ref, gain, bias, taps, shift,
+        q_hbm, k_hbm, v_hbm, g_hbm, res_hbm, ow_hbm, upg, upv, down,
+        out,
+        tapb, shiftb, wg, wd, qb, kb, vb, gb, ow, res, cum_col, st, lb, within,
+        xs, xr, dec, chain_s, chain_r, cb, cs, part, r1, s2, r2, acc, rows, ups, act,
+        load_sem, bulk_r, bulk_z, bulk_y, bulk_c, tap_s, tap_r, st_s, st_r, dec_s, dec_r, ch_s, ch_r, cb_s, cb_r,
+        rs1_s, rs1_r, rs2_s, rs2_r, ag_s, ag_r, halo_s, halo_r, f1_s, f1_r, f2_s, f2_r,
+    ):
+        sp, tp = lax.axis_index("sp"), lax.axis_index("tp")
+        z, y = sp // ny, sp % ny
+        x, c = tp // cores, tp % cores
+        me = z * ny + c
+        straight = c == y
+        crossed = jnp.logical_not(straight)
+        cross_sp, cross_tp = z * ny + c, x * cores + y
+        by_c = x * cores + 1 - c
+        by_x = (1 - x) * cores + c
+        by_y = z * ny + 1 - y
+
+        def remote(src, dst, ssem, rsem, to_sp, to_tp):
+            return pltpu.make_async_remote_copy(
+                src_ref=src, dst_ref=dst, send_sem=ssem, recv_sem=rsem,
+                device_id=(to_sp, to_tp), device_id_type=MESH,
+            )
+
+        def arrived(dst, ssem, rsem, cond=None):
+            copy = remote(dst, dst, ssem, rsem, sp, tp)
+            if cond is None:
+                copy.wait_recv()
+            else:
+                pl.when(cond)(copy.wait_recv)
+
+        own_rows = pl.ds(pl.multiple_of(tp * own, own), own)
+        pairs = [
+            (k_hbm, kb), (v_hbm, vb), (q_hbm, qb), (g_hbm, gb), (ow_hbm, ow), (res_hbm.at[own_rows], res),
+        ]
+        loads = [pltpu.make_async_copy(a, b, load_sem.at[i]) for i, (a, b) in enumerate(pairs)]
+        for load in loads:
+            load.start()
+        pairs = [(upg, wg.at[me, 0]), (upv, wg.at[me, 1]), (down, wd.at[me])]
+        weight_loads = [
+            pltpu.make_async_copy(a, b, load_sem.at[6 + i]) for i, (a, b) in enumerate(pairs)
+        ]
+        for load in weight_loads:
+            pl.when(straight)(load.start)
+
+        barrier = pltpu.get_barrier_semaphore()
+
+        def greet(to_sp, to_tp, cond=None):
+            def go():
+                pl.semaphore_signal(barrier, inc=1, device_id=(to_sp, to_tp), device_id_type=MESH)
+
+            if cond is None:
+                go()
+            else:
+                pl.when(cond)(go)
+
+        other_y = [z * ny + (y + d) % ny for d in range(1, ny)]
+        last_x = jnp.logical_and(c == 1, x == lines - 1)
+        next_sp = jnp.where(last_x, sp + 1, sp)
+        next_x = jnp.where(c == 0, x, jnp.where(last_x, 0, x + 1))
+        has_next = jnp.logical_or(jnp.logical_not(last_x), sp < n_sp - 1)
+        next_z = next_sp // ny
+        next_seg = next_sp % ny * lines + next_x
+        halo_to = [
+            (next_z * ny + yy, xx * cores + 1 - c, has_next) for yy in range(ny) for xx in range(lines)
+        ]
+        halo_from = []
+        for yy in range(ny):
+            for xx in range(lines):
+                here = z * ny + yy
+                if xx > 0:
+                    halo_from.append((here, jnp.where(c == 1, xx * cores, (xx - 1) * cores + 1), None))
+                else:
+                    halo_from.append(
+                        (
+                            jnp.where(c == 1, here, here - 1),
+                            jnp.where(c == 1, 0, (lines - 1) * cores + 1),
+                            jnp.logical_or(c == 1, here > 0),
+                        )
+                    )
+        other_c = [x * cores + (c + d) % cores for d in range(1, cores)]
+        other_x = [(x + d) % lines * cores + c for d in range(1, lines)]
+        peers = [(sp + ny, tp, z < nz - 1), (sp - ny, tp, z > 0)]
+        peers += [(o, tp, None) for o in other_y]
+        peers += [(sp, o, None) for o in other_c + other_x]
+        peers += [(cross_sp, cross_tp, crossed)]
+        peers += halo_to + halo_from
+        for to_sp, to_tp, cond in peers:
+            greet(to_sp, to_tp, cond)
+        count = jnp.int32(0)
+        for _, _, cond in peers:
+            count = count + (1 if cond is None else cond.astype(jnp.int32))
+        pl.semaphore_wait(barrier, count)
+
+        bulk = Sends()
+
+        def slot(p, src):
+            m, h = p // 2, p % 2
+            if m < 2:
+                return wg.at[src, m, pl.ds(h * dh, dh)]
+            return wd.at[src, pl.ds(h * hh, hh)]
+
+        def mine(p):
+            m, h = p // 2, p % 2
+            if m == 2:
+                return down.at[pl.ds(h * hh, hh)]
+            return (upg, upv)[m].at[pl.ds(h * dh, dh)]
+
+        def cross(p):
+            bulk.start(
+                remote(mine(p), slot(p, sp), bulk_y.at[p], bulk_r.at[p, sp], cross_sp, cross_tp), crossed
+            )
+
+        def own_z(p, up, also=None):
+            cond, to = (z < nz - 1, sp + ny) if up else (z > 0, sp - ny)
+            cond = jnp.logical_and(cond, straight)
+            if also is not None:
+                cond = jnp.logical_and(cond, also)
+            bulk.start(
+                remote(mine(p), slot(p, me), bulk_z.at[p, 0 if up else 1], bulk_r.at[p, me], to, tp),
+                cond,
+            )
+
+        def own_c(p):
+            bulk.start(
+                remote(mine(p), slot(p, me), bulk_c.at[p, 0], bulk_r.at[p, me], sp, by_c), straight
+            )
+
+        def crossed_own(p):
+            arrived(slot(p, me), bulk_y.at[p], bulk_r.at[p, me], crossed)
+            for up in (False, True):
+                cond, to = (z < nz - 1, sp + ny) if up else (z > 0, sp - ny)
+                bulk.start(
+                    remote(
+                        slot(p, me), slot(p, me), bulk_z.at[p, 2 if up else 3], bulk_r.at[p, me], to, tp
+                    ),
+                    jnp.logical_and(cond, crossed),
+                )
+            bulk.start(
+                remote(slot(p, me), slot(p, me), bulk_c.at[p, 1], bulk_r.at[p, me], sp, by_c), crossed
+            )
+
+        middle = jnp.logical_and(z > 0, z < nz - 1)
+
+        def source(up, d, also=None):
+            src, cond = (me - d * ny, z >= d) if up else (me + d * ny, z < nz - d)
+            return src, cond if also is None else jnp.logical_and(cond, also)
+
+        def take(p, up, d, also=None):
+            src, cond = source(up, d, also)
+            src = jnp.clip(src, 0, n_sp - 1)
+            arrived(slot(p, src), bulk_z.at[p, 0], bulk_r.at[p, src], cond)
+
+        def on_z(p, up, d, also=None):
+            src, cond = source(up, d, also)
+            src = jnp.clip(src, 0, n_sp - 1)
+            to, more = (sp + ny, z < nz - 1) if up else (sp - ny, z > 0)
+            sem = bulk_z.at[p, 2 + 2 * d + (0 if up else 1)]
+            bulk.start(
+                remote(slot(p, src), slot(p, src), sem, bulk_r.at[p, src], to, tp),
+                jnp.logical_and(cond, more),
+            )
+
+        def on_c(p, up, d, also=None):
+            src, cond = source(up, d, also)
+            src = jnp.clip(src, 0, n_sp - 1)
+            sem = bulk_c.at[p, 2 * d + (0 if up else 1)]
+            bulk.start(
+                remote(slot(p, src), slot(p, src), sem, bulk_r.at[p, src], sp, by_c), cond
+            )
+
+        def relay(m, up, d, also=None):
+            if d >= nz:
+                return
+            for p in (2 * m, 2 * m + 1):
+                take(p, up, d, also)
+                if d < nz - 1:
+                    on_z(p, up, d, also)
+                on_c(p, up, d, also)
+
+        def side_arrivals(m):
+            for zz in range(nz):
+                for p in (2 * m, 2 * m + 1):
+                    src = zz * ny + 1 - c
+                    arrived(slot(p, src), bulk_z.at[p, 0], bulk_r.at[p, src])
+
+        own_z(0, True)
+        own_z(1, True, z > 0)
+        for p in (0, 1, 2, 3):
+            own_z(p, False)
+
+        ii = lax.broadcasted_iota(jnp.int32, (BLOCK, BLOCK), 0)
+        jj = lax.broadcasted_iota(jnp.int32, (BLOCK, BLOCK), 1)
+        lower = (ii >= jj).astype(F32)
+        logs = log_ref[...]
+        cum_col[...] = dot_t(lower, logs, ((1,), (1,)), lax.Precision.HIGHEST)
+
+        def column(idx):
+            lane = lax.broadcasted_iota(jnp.int32, cum_col.shape, 1)
+            return jnp.sum(jnp.where(lane == idx, cum_col[...], 0.0), axis=1, keepdims=True)
+
+        def angles(b):
+            row = pl.ds(sp * nb + b, 1)
+            co, so = cos_out[row, :], sin_out[row, :]
+            ci, si = cos_in[...], sin_in[...]
+            return ci * co - si * so, si * co + ci * so
+
+        def rotated(value, cosine, sine):
+            front, second = value[:, :half_k], value[:, half_k:]
+            return jnp.concatenate(
+                [front * cosine - second * sine, front * sine + second * cosine], axis=1
+            )
+
+        def block_rows(b):
+            return pl.ds(pl.multiple_of(b * BLOCK, BLOCK), BLOCK)
+
+        loads[0].wait()
+        loads[1].wait()
+        st[...] = jnp.zeros_like(st)
+
+        def local_states(b, _):
+            r = block_rows(b)
+            cosine, sine = angles(b)
+            for h in range(heads):
+                cc = column(h * nb + b)
+                total = cc[BLOCK - 1 : BLOCK, :]
+                kc = pl.ds(h * key_width, key_width)
+                key = rotated(kb[r, kc].astype(F32), cosine, sine) * key_width ** (-0.5)
+                key = key.astype(BF16)
+                kb[r, kc] = key
+                faded = (key.astype(F32) * jnp.exp(total - cc)).astype(BF16)
+                term = dot_t(faded, vb[r, pl.ds(h * value_width, value_width)], ((0,), (0,)))
+                before = st[h]
+                lb[b * heads + h] = before.astype(BF16)
+                st[h] = jnp.exp(total) * before + term
+            return 0
+
+        lax.fori_loop(0, nb, local_states, 0)
+
+        def head_log(h):
+            total = jnp.zeros((1, 1), F32)
+            for b in range(nb):
+                total = total + jnp.sum(logs[h * nb + b : h * nb + b + 1, :], axis=1, keepdims=True)
+            return total
+
+        hrow = lax.broadcasted_iota(jnp.int32, (8, 128), 0)
+        tile = jnp.zeros((8, 128), F32)
+        for h in range(heads):
+            tile = jnp.where(hrow == h, head_log(h), tile)
+        dec[pl.ds(y, 1)] = tile[None]
+        states = Sends()
+        for d, to in enumerate(other_y):
+            far = (y + d + 1) % ny
+            states.start(
+                remote(dec.at[y], dec.at[y], dec_s.at[d], dec_r.at[y], to, tp)
+            )
+            for h in range(heads):
+                for f in range(ny):
+
+                    @pl.when(far == f)
+                    def _():
+                        xs[d, h] = st[h, :, f * slice_w : (f + 1) * slice_w].astype(BF16)
+
+                states.start(
+                    remote(xs.at[d, h], xr.at[y, h], st_s.at[d, h], st_r.at[y, h], to, tp)
+                )
+        cross(0)
+        cross(1)
+
+        loads[2].wait()
+
+        def within_block(b, _):
+            r = block_rows(b)
+            cosine, sine = angles(b)
+            for h in range(heads):
+                cc = column(h * nb + b)
+                kc = pl.ds(h * key_width, key_width)
+                query = rotated(qb[r, kc].astype(F32), cosine, sine).astype(BF16)
+                scores = dot_t(query, kb[r, kc], ((1,), (1,)))
+                crow = jnp.sum(jnp.where(ii == jj, cc, 0.0), axis=0, keepdims=True)
+                gap = jnp.where(ii >= jj, cc - crow, 0.0)
+                weight = jnp.where(ii >= jj, jnp.exp(gap), 0.0)
+                vc = pl.ds(h * value_width, value_width)
+                within[r, vc] = dot((scores * weight).astype(BF16), vb[r, vc])
+                qb[r, kc] = (query.astype(F32) * jnp.exp(cc)).astype(BF16)
+            return 0
+
+        lax.fori_loop(0, nb, within_block, 0)
+
+        for f in range(ny):
+
+            @pl.when(y == f)
+            def _():
+                for h in range(heads):
+                    xr[f, h] = st[h, :, f * slice_w : (f + 1) * slice_w].astype(BF16)
+
+        for d in range(1, ny):
+            src = (y + d) % ny
+            arrived(dec.at[src], dec_s.at[0], dec_r.at[src])
+            for h in range(heads):
+                arrived(xr.at[src, h], st_s.at[0, 0], st_r.at[src, h])
+        for h in range(heads):
+
+            @pl.when(z == 0)
+            def _():
+                chain_r[h] = jnp.zeros((key_width, slice_w), BF16)
+
+            arrived(chain_r.at[h], ch_s.at[h], ch_r.at[h], z > 0)
+            incoming = chain_r[h].astype(F32)
+            before = incoming
+            for f in range(ny):
+                cb_mine = before.astype(BF16)
+
+                @pl.when(y == f)
+                def _():
+                    cb[y, h] = cb_mine
+
+                @pl.when(y != f)
+                def _():
+                    cs[f, h] = cb_mine
+
+                decay = jnp.exp(dec[f, h : h + 1, 0:1])
+                before = decay * before + xr[f, h].astype(F32)
+            chain_s[h] = before.astype(BF16)
+            states.start(
+                remote(chain_s.at[h], chain_r.at[h], ch_s.at[h], ch_r.at[h], sp + ny, tp),
+                z < nz - 1,
+            )
+            for d, to in enumerate(other_y):
+                far = (y + d + 1) % ny
+                states.start(
+                    remote(cs.at[far, h], cb.at[y, h], cb_s.at[d, h], cb_r.at[y, h], to, tp)
+                )
+
+        own_z(1, True, z == 0)
+        for p in (2, 3):
+            own_z(p, True)
+        for p in range(4):
+            own_c(p)
+        for p in (2, 3, 4, 5):
+            cross(p)
+        bulk.start(remote(taps, tapb, tap_s.at[0], tap_r.at[0], cross_sp, cross_tp), crossed)
+        bulk.start(remote(shift, shiftb, tap_s.at[1], tap_r.at[1], cross_sp, cross_tp), crossed)
+
+        @pl.when(straight)
+        def _():
+            tapb[...] = taps[...]
+            shiftb[...] = shift[...]
+
+        crossed_own(0)
+        crossed_own(1)
+        relay(0, False, 1, straight)
+
+        loads[3].wait()
+        for h in range(heads):
+            for d in range(1, ny):
+                src = (y + d) % ny
+                arrived(cb.at[src, h], cb_s.at[0, 0], cb_r.at[src, h])
+
+            def finish(b, decay):
+                r = block_rows(b)
+                vc = pl.ds(h * value_width, value_width)
+                state = jnp.concatenate([cb[f, h].astype(F32) for f in range(ny)], axis=1)
+                state = (decay * state + lb[b * heads + h].astype(F32)).astype(BF16)
+                mixed = within[r, vc] + dot(qb[r, pl.ds(h * key_width, key_width)], state)
+                average = jnp.mean(mixed, axis=1, keepdims=True)
+                mixed = mixed - average
+                spread = jnp.mean(mixed * mixed, axis=1, keepdims=True)
+                gate = gb[r, vc].astype(F32)
+                gated = gate * jax.nn.sigmoid(gate) * (mixed * lax.rsqrt(spread + tiny_stabilizer))
+                gb[r, vc] = gated.astype(BF16)
+                return decay * jnp.exp(column(h * nb + b)[BLOCK - 1 : BLOCK, :])
+
+            lax.fori_loop(0, nb, finish, jnp.ones((1, 1), F32))
+        states.drain()
+
+        def owner_rows(xx, cc):
+            return pl.ds(pl.multiple_of((xx * cores + cc) * own, own), own)
+
+        def piece_cols(s):
+            return pl.ds(pl.multiple_of(s * piece, piece), piece)
+
+        def d2d_copies(s):
+            return [
+                remote(
+                    part.at[s, owner_rows(xx, (c + d) % cores)], r1.at[s, d - 1, xx],
+                    rs1_s.at[s, d - 1, xx], rs1_r.at[s, d - 1, xx],
+                    sp, x * cores + (c + d) % cores,
+                )
+                for d in range(1, cores)
+                for xx in range(lines)
+            ]
+
+        def x_copies(s):
+            return [
+                remote(
+                    s2.at[s, d - 1], r2.at[s, d - 1], rs2_s.at[s, d - 1], rs2_r.at[s, d - 1],
+                    sp, (x + d) % lines * cores + c,
+                )
+                for d in range(1, lines)
+            ]
+
+        row_tile = min(tok_rows, 512)
+
+        def product(s, lhs, rhs):
+            def one(i, _):
+                r = pl.ds(pl.multiple_of(i * row_tile, row_tile), row_tile)
+                part[s, r, :] = dot(lhs[r, :], rhs()).astype(BF16)
+                return 0
+
+            lax.fori_loop(0, tok_rows // row_tile, one, 0)
+            for copy in d2d_copies(s):
+                copy.start()
+
+        def combine(s):
+            for copy in d2d_copies(s):
+                copy.wait_recv()
+            for d in range(lines):
+                xx = (x + d) % lines
+                total = part[s, owner_rows(xx, c), :].astype(F32)
+                for e in range(cores - 1):
+                    total = total + r1[s, e, xx].astype(F32)
+                if d == 0:
+                    acc[:, piece_cols(s)] = total
+                else:
+                    s2[s, d - 1] = total.astype(BF16)
+            for copy in x_copies(s):
+                copy.start()
+
+        def collect(s):
+            for copy in x_copies(s):
+                copy.wait_recv()
+            total = acc[:, piece_cols(s)]
+            for d in range(lines - 1):
+                total = total + r2[s, d].astype(F32)
+            acc[:, piece_cols(s)] = total
+
+        def release(s, _):
+            for copy in d2d_copies(s) + x_copies(s):
+                copy.wait_send()
+            return 0
+
+        def out_step(s, _):
+            product(s, gb, lambda: ow[:, piece_cols(s)])
+            pl.when(s > 0)(lambda: combine(s - 1))
+            return 0
+
+        loads[4].wait()
+        lax.fori_loop(0, n_sp, out_step, 0)
+        combine(n_sp - 1)
+        crossed_own(2)
+        crossed_own(3)
+        relay(0, False, 1, crossed)
+        relay(0, True, 1)
+        relay(0, False, 2)
+        relay(0, True, 2)
+        relay(1, False, 1)
+        relay(1, True, 1)
+
+        def collect_step(s, _):
+            collect(s)
+            return 0
+
+        lax.fori_loop(0, n_sp, collect_step, 0)
+
+        loads[5].wait()
+
+        def layer_norm(values, which):
+            average = jnp.mean(values, axis=1, keepdims=True)
+            values = values - average
+            spread = jnp.mean(values * values, axis=1, keepdims=True)
+            values = values * lax.rsqrt(spread + tiny_stabilizer)
+            return values * gain[which : which + 1, :] + bias[which : which + 1, :]
+
+        ln_rows = 32
+        gathered = Sends()
+
+        seg = HALO + own
+
+        def chunk_of(yy, xx, j):
+            at = (yy * lines + xx) * seg + HALO + j * chunk
+            return rows.at[pl.ds(pl.multiple_of(at, 16), chunk)]
+
+        def gather_sem(j, yy, xx):
+            return ag_r.at[j, yy * lines + xx]
+
+        for yy in range(ny):
+            for xx in range(lines):
+                if yy == 0 and xx == 0:
+
+                    @pl.when(jnp.logical_and(z == 0, c == 0))
+                    def _():
+                        rows[pl.ds(0, HALO), :] = jnp.zeros((HALO, width), BF16)
+
+        for j in range(ROW_CHUNKS):
+
+            def norm_rows(i, _):
+                at = pl.multiple_of(j * chunk + i * ln_rows, ln_rows)
+                r = pl.ds(at, ln_rows)
+                value = layer_norm(alpha_scale * res[r, :].astype(F32) + acc[r, :], 0).astype(BF16)
+                res[r, :] = value
+                rows[pl.ds(pl.multiple_of((y * lines + x) * seg + HALO + at, 16), ln_rows), :] = value
+                return 0
+
+            lax.fori_loop(0, chunk // ln_rows, norm_rows, 0)
+            mine_now = chunk_of(y, x, j)
+            gathered.start(remote(mine_now, mine_now, ag_s.at[j, 0], gather_sem(j, y, x), sp, by_x))
+            gathered.start(remote(mine_now, mine_now, ag_s.at[j, 1], gather_sem(j, y, x), by_y, tp))
+        tail = rows.at[pl.ds(pl.multiple_of((y * lines + x) * seg + own, 16), HALO)]
+        head = rows.at[pl.ds(pl.multiple_of(next_seg * seg, 16), HALO)]
+        for t, (to_sp, to_tp, cond) in enumerate(halo_to):
+            gathered.start(remote(tail, head, halo_s.at[t], halo_r.at[next_seg], to_sp, to_tp), cond)
+        for j in range(ROW_CHUNKS):
+            if j == ROW_CHUNKS // 2:
+                relay(0, False, 3)
+                relay(1, False, 2, z > 0)
+                relay(1, True, 2, z < nz - 1)
+            if j == ROW_CHUNKS - 1:
+                relay(0, True, 3)
+            got = chunk_of(y, 1 - x, j)
+            arrived(got, ag_s.at[j, 0], gather_sem(j, y, 1 - x))
+            if j % 2 == 0:
+                gathered.start(remote(got, got, ag_s.at[j, 2], gather_sem(j, y, 1 - x), by_y, tp))
+            got = chunk_of(1 - y, x, j)
+            arrived(got, ag_s.at[j, 0], gather_sem(j, 1 - y, x))
+            if j % 2 == 1:
+                gathered.start(remote(got, got, ag_s.at[j, 2], gather_sem(j, 1 - y, x), sp, by_x))
+        for p in (4, 5):
+            own_z(p, False)
+            own_z(p, True)
+            own_c(p)
+            crossed_own(p)
+        for j in range(ROW_CHUNKS):
+            arrived(chunk_of(1 - y, 1 - x, j), ag_s.at[j, 0], gather_sem(j, 1 - y, 1 - x))
+        relay(1, False, 2, z == 0)
+        relay(1, True, 2, z == nz - 1)
+        for d in range(4, nz):
+            relay(0, False, d)
+            relay(0, True, d)
+        lax.fori_loop(0, n_sp, release, 0)
+
+        def up_tile(m, start, count):
+            r = pl.ds(start, count)
+            total = None
+            for s in range(n_sp):
+                term = dot(rows[r, s * depth : (s + 1) * depth], wg[s, m])
+                total = term if total is None else total + term
+            ups[m, r, :] = total.astype(BF16)
+
+        def up_rows(m):
+            def one(i, _):
+                up_tile(m, pl.multiple_of(i * seg, 16), seg)
+                return 0
+
+            lax.fori_loop(0, n_tp, one, 0)
+
+        pl.when(straight)(weight_loads[0].wait)
+        side_arrivals(0)
+        for g, (_, _, cond) in enumerate(halo_from):
+            arrived(rows.at[pl.ds(g * seg, HALO)], halo_s.at[0], halo_r.at[g], cond)
+        up_rows(0)
+        for d in range(3, nz):
+            relay(1, False, d)
+            relay(1, True, d)
+        relay(2, False, 1, middle)
+        relay(2, True, 1, middle)
+        pl.when(straight)(weight_loads[1].wait)
+        side_arrivals(1)
+        up_rows(1)
+
+        arrived(tapb, tap_s.at[0], tap_r.at[0], crossed)
+        arrived(shiftb, tap_s.at[1], tap_r.at[1], crossed)
+
+        def activate(i, col):
+            at = pl.multiple_of(i * seg, 16)
+            convs = []
+            for m in range(2):
+                tile = ups[m, pl.ds(at, seg), col].astype(F32)
+                value = shiftb[m : m + 1, col]
+                for j in range(3):
+                    value = value + tapb[m, j : j + 1, col] * tile[HALO - 2 + j : HALO - 2 + j + own, :]
+                convs.append(value)
+            act[pl.ds(pl.multiple_of(i * own, 16), own), col] = (
+                jax.nn.gelu(convs[0]) * convs[1]
+            ).astype(BF16)
+
+        def activate_step(i, _):
+            for t in range(hidden // hcols):
+                activate(i, pl.ds(t * hcols, hcols))
+            return 0
+
+        lax.fori_loop(0, n_tp, activate_step, 0)
+
+        order = [
+            [zz] + sorted((o for o in range(nz) if o != zz), key=lambda o: (abs(o - zz), abs(2 * o - nz + 1)))
+            for zz in range(nz)
+        ]
+
+        def nearest(k):
+            got = jnp.int32(order[0][k])
+            for zz in range(1, nz):
+                got = jnp.where(z == zz, order[zz][k], got)
+            return got
+
+        half = piece // 2
+        left, right = pl.ds(0, half), pl.ds(half, half)
+
+        def seg_rows(yy, xx):
+            return pl.ds(pl.multiple_of((yy * lines + xx) * own, own), own)
+
+        def first_hops(s):
+            copies = [
+                remote(
+                    part.at[s, seg_rows(yy, 1 - x), left], r1.at[s, 0, yy, :, left],
+                    f1_s.at[s, yy], f1_r.at[s, yy], sp, by_x,
+                )
+                for yy in range(ny)
+            ]
+            return copies + [
+                remote(
+                    part.at[s, seg_rows(1 - y, xx), right], r1.at[s, 0, xx, :, right],
+                    f1_s.at[s, ny + xx], f1_r.at[s, ny + xx], by_y, tp,
+                )
+                for xx in range(lines)
+            ]
+
+        def second_hops(s):
+            return [
+                remote(
+                    s2.at[s, 0, :, left], r2.at[s, 0, :, left], f2_s.at[s, 0], f2_r.at[s, 0], by_y, tp
+                ),
+                remote(
+                    s2.at[s, 0, :, right], r2.at[s, 0, :, right], f2_s.at[s, 1], f2_r.at[s, 1], sp, by_x
+                ),
+            ]
+
+        def halves(s):
+            at = pl.multiple_of(s * piece, piece)
+            return pl.ds(at, half), pl.ds(pl.multiple_of(at + half, half), half)
+
+        def down_step(s):
+            def one(i, _):
+                r = pl.ds(pl.multiple_of(i * row_tile, row_tile), row_tile)
+                part[s, r, :] = dot(act[r, :], wd[s]).astype(BF16)
+                return 0
+
+            lax.fori_loop(0, tok_rows // row_tile, one, 0)
+            for copy in first_hops(s):
+                copy.start()
+
+        def down_combine(s):
+            for copy in first_hops(s):
+                copy.wait_recv()
+            lcols, rcols = halves(s)
+
+            def summed(yy, xx, other, cols):
+                return part[s, seg_rows(yy, xx), cols].astype(F32) + r1[s, 0, other, :, cols].astype(F32)
+
+            s2[s, 0, :, left] = summed(1 - y, x, 1 - y, left).astype(BF16)
+            s2[s, 0, :, right] = summed(y, 1 - x, 1 - x, right).astype(BF16)
+            for copy in second_hops(s):
+                copy.start()
+            acc[:, lcols] = summed(y, x, y, left)
+            acc[:, rcols] = summed(y, x, x, right)
+
+        def down_collect(s):
+            for copy in second_hops(s):
+                copy.wait_recv()
+            acc[:, piece_cols(s)] = acc[:, piece_cols(s)] + r2[s, 0].astype(F32)
+
+        def down_release(s, _):
+            for copy in first_hops(s) + second_hops(s):
+                copy.wait_send()
+            return 0
+
+        pl.when(straight)(weight_loads[2].wait)
+        previous = None
+        done = []
+        for k in range(nz):
+            src_z = nearest(k)
+            if k > 0:
+                src = src_z * ny + c
+                to_z = jnp.where(src_z < z, z + 1, z - 1)
+                more = jnp.logical_and(to_z >= 0, to_z < nz)
+                fresh = jnp.logical_not(jnp.logical_and(middle, jnp.abs(src_z - z) == 1))
+                for p in (4, 5):
+                    arrived(slot(p, src), bulk_z.at[p, 0], bulk_r.at[p, src], fresh)
+                    bulk.start(
+                        remote(
+                            slot(p, src), slot(p, src), bulk_z.at[p, 2 * nz + 2 + k],
+                            bulk_r.at[p, src], to_z * ny + y, tp,
+                        ),
+                        jnp.logical_and(more, fresh),
+                    )
+                    bulk.start(
+                        remote(
+                            slot(p, src), slot(p, src), bulk_c.at[p, 2 * nz + k],
+                            bulk_r.at[p, src], sp, by_c,
+                        ),
+                        fresh,
+                    )
+            for d in range(cores):
+                src = src_z * ny + (c + d) % cores
+                if d > 0:
+                    for p in (4, 5):
+                        arrived(slot(p, src), bulk_z.at[p, 0], bulk_r.at[p, src])
+                down_step(src)
+                if previous is not None:
+                    down_combine(previous)
+                previous = src
+                done.append(src)
+        down_combine(previous)
+        for src in done:
+            down_collect(src)
+
+        def final_rows(i, _):
+            r = pl.ds(pl.multiple_of(i * ln_rows, ln_rows), ln_rows)
+            out[r, :] = layer_norm(alpha_scale * res[r, :].astype(F32) + acc[r, :], 1).astype(BF16)
+            return 0
+
+        lax.fori_loop(0, own // ln_rows, final_rows, 0)
+        lax.fori_loop(0, n_sp, down_release, 0)
+        gathered.drain()
+        bulk.drain()
+
+    vmem, dma = pltpu.VMEM, pltpu.SemaphoreType.DMA
+    oc, ol, oy = max(cores - 1, 1), max(lines - 1, 1), max(ny - 1, 1)
+    scratch = [
+        vmem((2, 3, hidden), F32),
+        vmem((2, hidden), F32),
+        vmem((n_sp, 2, depth, hidden), BF16),
+        vmem((n_sp, hidden, piece), BF16),
+        vmem((tok_rows, heads * key_width), BF16),
+        vmem((tok_rows, heads * key_width), BF16),
+        vmem((tok_rows, heads * value_width), BF16),
+        vmem((tok_rows, heads * value_width), BF16),
+        vmem((heads * value_width, width), BF16),
+        vmem((own, width), BF16),
+        vmem((BLOCK, heads * nb), F32),
+        vmem((heads, key_width, value_width), F32),
+        vmem((nb * heads, key_width, value_width), BF16),
+        vmem((tok_rows, heads * value_width), F32),
+        vmem((oy, heads, key_width, slice_w), BF16),
+        vmem((ny, heads, key_width, slice_w), BF16),
+        vmem((ny, 8, 128), F32),
+        vmem((heads, key_width, slice_w), BF16),
+        vmem((heads, key_width, slice_w), BF16),
+        vmem((ny, heads, key_width, slice_w), BF16),
+        vmem((ny, heads, key_width, slice_w), BF16),
+        vmem((n_sp, tok_rows, piece), BF16),
+        vmem((n_sp, oc, lines, own, piece), BF16),
+        vmem((n_sp, ol, own, piece), BF16),
+        vmem((n_sp, ol, own, piece), BF16),
+        vmem((own, width), F32),
+        vmem((n_tp * HALO + tok_rows, width), BF16),
+        vmem((2, n_tp * HALO + tok_rows, hidden), BF16),
+        vmem((tok_rows, hidden), BF16),
+        dma((9,)),
+        dma((6, n_sp)),
+        dma((6, 3 * nz + 2)),
+        dma((6,)),
+        dma((6, 3 * nz)),
+        dma((2,)),
+        dma((2,)),
+        dma((oy, heads)),
+        dma((ny, heads)),
+        dma((oy,)),
+        dma((ny,)),
+        dma((heads,)),
+        dma((heads,)),
+        dma((oy, heads)),
+        dma((ny, heads)),
+        dma((n_sp, oc, lines)),
+        dma((n_sp, oc, lines)),
+        dma((n_sp, ol)),
+        dma((n_sp, ol)),
+        dma((ROW_CHUNKS, 3)),
+        dma((ROW_CHUNKS, n_tp)),
+        dma((n_tp,)),
+        dma((n_tp,)),
+        dma((n_sp, ny + lines)),
+        dma((n_sp, ny + lines)),
+        dma((n_sp, 2)),
+        dma((n_sp, 2)),
+    ]
+    in_specs = [pl.BlockSpec(memory_space=pltpu.VMEM)] * 9 + [pl.BlockSpec(memory_space=pl.ANY)] * 9
+    return pl.pallas_call(
+        kernel,
+        out_shape=jax.ShapeDtypeStruct((own, width), BF16),
+        in_specs=in_specs,
+        out_specs=pl.BlockSpec(memory_space=pltpu.VMEM),
+        scratch_shapes=scratch,
+        compiler_params=pltpu.CompilerParams(
+            collective_id=0, has_side_effects=True, vmem_limit_bytes=67_000_000
+        ),
+    )
+
+
 def shards(
     query_proj, key_proj, value_proj, gate_proj, log_decay, residual, out_weight, norm_gain,
     norm_bias, up_gate, up_value, conv_weight, conv_bias, down_weight,
@@ -772,7 +1583,9 @@
     key_width = query_proj.shape[1] // heads
     value_width = value_proj.shape[1] // heads
     nb = tok_rows // BLOCK
-    call = make_kernel(
+    cores, lines, ny, _ = layout(n_sp, n_tp)
+    make = make_square_kernel if cores == lines == ny == 2 else make_kernel
+    call = make(
         n_sp, n_tp, tok_rows, heads, key_width, value_width,
         residual.shape[1], up_gate.shape[0], up_gate.shape[1],
     )

time: 211 us -> 189 us (0.90)
  Pallas kernels: 206 us -> 183 us
    pallas_call x1, Pallas kernels: 206 us -> 183 us  [shards(): call(*tables, logs, norm_gain, norm_bias, conv_weight, conv_bias, query_p...]
where the time goes in v2:
time: 189 us; the launch traced here: 188 us
  Pallas kernels  183 us (97%)
  local copies, waits for them, and re-layouts  4.99 us (3%)
    pallas_call x1, Pallas kernels, shards(): call(*tables, logs, norm_gain, norm_bias, conv_weight, conv_bias, query_p...  183 us

profile of v2, /device:TPU:30, one launch (start us, length us, event | category | flops | bytes accessed | tf_op | source)
XLA Modules:
  0.0 188.1 jit_solution(2898930265888863878)
XLA Ops:
  0.0 1.3 reshape.3.log_ref
  1.3 1.4 copy.19.taps
  2.7 183.1 %shard_map.172 = bf16[256,2048]{1,0:T(8,128)(2,1)} custom-call(f32[256,128]{1,0:T(8,128)} %constant.8.clone.cos_in, f32[256,128]{1,0:T(8,128)} %constant.9.clone.sin_in, f32[32,128]{1,0:T(8,128)} %constant.10.clone.cos_out, f32[32,128]{1,0:T(8,128)} %constant.11.clone.sin_out, f32[8,256]{1,0:T(8,128)} %reshape.3.log_ref, f32[2,2048]{1,0:T(2,128)} %gain.1, ...), custom_call_target="tpu_custom_call" | custom-call | tf_op jit(solution)/shard_map/pallas_call | solution.py:1594
  185.8 2.3 %copy.21 = bf16[256,2048]{1,0:T(8,128)(2,1)} copy(bf16[256,2048]{1,0:T(8,128)(2,1)} %shard_map.172) | data formatting | bytes 2097152

commit v3 on v2

--- a/solution.py
+++ b/solution.py
@@ -781,7 +781,7 @@
         tapb, shiftb, wg, wd, qb, kb, vb, gb, ow, res, cum_col, st, lb, within,
         xs, xr, dec, chain_s, chain_r, cb, cs, part, r1, s2, r2, acc, rows, ups, act,
         load_sem, bulk_r, bulk_z, bulk_y, bulk_c, tap_s, tap_r, st_s, st_r, dec_s, dec_r, ch_s, ch_r, cb_s, cb_r,
-        rs1_s, rs1_r, rs2_s, rs2_r, ag_s, ag_r, halo_s, halo_r, f1_s, f1_r, f2_s, f2_r,
+        ag_s, ag_r, halo_s, halo_r, f1_s, f1_r, f2_s, f2_r,
     ):
         sp, tp = lax.axis_index("sp"), lax.axis_index("tp")
         z, y = sp // ny, sp % ny
@@ -884,9 +884,10 @@
                 return down.at[pl.ds(h * hh, hh)]
             return (upg, upv)[m].at[pl.ds(h * dh, dh)]
 
-        def cross(p):
+        def cross(p, also=None):
+            cond = crossed if also is None else jnp.logical_and(crossed, also)
             bulk.start(
-                remote(mine(p), slot(p, sp), bulk_y.at[p], bulk_r.at[p, sp], cross_sp, cross_tp), crossed
+                remote(mine(p), slot(p, sp), bulk_y.at[p], bulk_r.at[p, sp], cross_sp, cross_tp), cond
             )
 
         def own_z(p, up, also=None):
@@ -895,27 +896,28 @@
             if also is not None:
                 cond = jnp.logical_and(cond, also)
             bulk.start(
-                remote(mine(p), slot(p, me), bulk_z.at[p, 0 if up else 1], bulk_r.at[p, me], to, tp),
+                remote(mine(p), slot(p, me), bulk_z.at[p, z if up else nz], bulk_r.at[p, me], to, tp),
                 cond,
             )
 
         def own_c(p):
             bulk.start(
-                remote(mine(p), slot(p, me), bulk_c.at[p, 0], bulk_r.at[p, me], sp, by_c), straight
-            )
-
-        def crossed_own(p):
-            arrived(slot(p, me), bulk_y.at[p], bulk_r.at[p, me], crossed)
+                remote(mine(p), slot(p, me), bulk_c.at[p, z], bulk_r.at[p, me], sp, by_c), straight
+            )
+
+        def crossed_own(p, also=None):
+            go = crossed if also is None else jnp.logical_and(crossed, also)
+            arrived(slot(p, me), bulk_y.at[p], bulk_r.at[p, me], go)
             for up in (False, True):
                 cond, to = (z < nz - 1, sp + ny) if up else (z > 0, sp - ny)
                 bulk.start(
                     remote(
-                        slot(p, me), slot(p, me), bulk_z.at[p, 2 if up else 3], bulk_r.at[p, me], to, tp
+                        slot(p, me), slot(p, me), bulk_z.at[p, z if up else nz], bulk_r.at[p, me], to, tp
                     ),
-                    jnp.logical_and(cond, crossed),
+                    jnp.logical_and(cond, go),
                 )
             bulk.start(
-                remote(slot(p, me), slot(p, me), bulk_c.at[p, 1], bulk_r.at[p, me], sp, by_c), crossed
+                remote(slot(p, me), slot(p, me), bulk_c.at[p, z], bulk_r.at[p, me], sp, by_c), go
             )
 
         middle = jnp.logical_and(z > 0, z < nz - 1)
@@ -933,7 +935,7 @@
             src, cond = source(up, d, also)
             src = jnp.clip(src, 0, n_sp - 1)
             to, more = (sp + ny, z < nz - 1) if up else (sp - ny, z > 0)
-            sem = bulk_z.at[p, 2 + 2 * d + (0 if up else 1)]
+            sem = bulk_z.at[p, src // ny]
             bulk.start(
                 remote(slot(p, src), slot(p, src), sem, bulk_r.at[p, src], to, tp),
                 jnp.logical_and(cond, more),
@@ -942,7 +944,7 @@
         def on_c(p, up, d, also=None):
             src, cond = source(up, d, also)
             src = jnp.clip(src, 0, n_sp - 1)
-            sem = bulk_c.at[p, 2 * d + (0 if up else 1)]
+            sem = bulk_c.at[p, src // ny]
             bulk.start(
                 remote(slot(p, src), slot(p, src), sem, bulk_r.at[p, src], sp, by_c), cond
             )
@@ -964,8 +966,11 @@
 
         own_z(0, True)
         own_z(1, True, z > 0)
+        own_z(2, True, z > 0)
+        own_z(3, True, z > 1)
         for p in (0, 1, 2, 3):
             own_z(p, False)
+        cross(0)
 
         ii = lax.broadcasted_iota(jnp.int32, (BLOCK, BLOCK), 0)
         jj = lax.broadcasted_iota(jnp.int32, (BLOCK, BLOCK), 1)
@@ -1042,8 +1047,10 @@
                 states.start(
                     remote(xs.at[d, h], xr.at[y, h], st_s.at[d, h], st_r.at[y, h], to, tp)
                 )
-        cross(0)
         cross(1)
+        upper = z >= nz // 2
+        cross(2, upper)
+        cross(3, upper)
 
         loads[2].wait()
 
@@ -1064,6 +1071,7 @@
             return 0
 
         lax.fori_loop(0, nb, within_block, 0)
+        crossed_own(0)
 
         for f in range(ny):
 
@@ -1077,6 +1085,7 @@
             arrived(dec.at[src], dec_s.at[0], dec_r.at[src])
             for h in range(heads):
                 arrived(xr.at[src, h], st_s.at[0, 0], st_r.at[src, h])
+        crossed_own(1, upper)
         for h in range(heads):
 
             @pl.when(z == 0)
@@ -1111,11 +1120,13 @@
                 )
 
         own_z(1, True, z == 0)
-        for p in (2, 3):
-            own_z(p, True)
+        own_z(2, True, z == 0)
+        own_z(3, True, z <= 1)
         for p in range(4):
             own_c(p)
-        for p in (2, 3, 4, 5):
+        for p in (2, 3):
+            cross(p, jnp.logical_not(upper))
+        for p in (4, 5):
             cross(p)
         bulk.start(remote(taps, tapb, tap_s.at[0], tap_r.at[0], cross_sp, cross_tp), crossed)
         bulk.start(remote(shift, shiftb, tap_s.at[1], tap_r.at[1], cross_sp, cross_tp), crossed)
@@ -1125,9 +1136,14 @@
             tapb[...] = taps[...]
             shiftb[...] = shift[...]
 
-        crossed_own(0)
-        crossed_own(1)
+        crossed_own(1, jnp.logical_not(upper))
+        crossed_own(2, upper)
+        crossed_own(3, upper)
         relay(0, False, 1, straight)
+        for p in (4, 5):
+            own_z(p, False)
+            own_z(p, True)
+            own_c(p)
 
         loads[3].wait()
         for h in range(heads):
@@ -1162,7 +1178,7 @@
             return [
                 remote(
                     part.at[s, owner_rows(xx, (c + d) % cores)], r1.at[s, d - 1, xx],
-                    rs1_s.at[s, d - 1, xx], rs1_r.at[s, d - 1, xx],
+                    f1_s.at[s, (d - 1) * lines + xx], f1_r.at[s, (d - 1) * lines + xx],
                     sp, x * cores + (c + d) % cores,
                 )
                 for d in range(1, cores)
@@ -1172,7 +1188,7 @@
         def x_copies(s):
             return [
                 remote(
-                    s2.at[s, d - 1], r2.at[s, d - 1], rs2_s.at[s, d - 1], rs2_r.at[s, d - 1],
+                    s2.at[s, d - 1], r2.at[s, d - 1], f2_s.at[s, d - 1], f2_r.at[s, d - 1],
                     sp, (x + d) % lines * cores + c,
                 )
                 for d in range(1, lines)
@@ -1226,14 +1242,14 @@
         loads[4].wait()
         lax.fori_loop(0, n_sp, out_step, 0)
         combine(n_sp - 1)
-        crossed_own(2)
-        crossed_own(3)
+        crossed_own(2, jnp.logical_not(upper))
+        crossed_own(3, jnp.logical_not(upper))
         relay(0, False, 1, crossed)
         relay(0, True, 1)
-        relay(0, False, 2)
-        relay(0, True, 2)
-        relay(1, False, 1)
-        relay(1, True, 1)
+        relay(0, False, 2, straight)
+        relay(0, True, 2, straight)
+        relay(1, False, 1, straight)
+        relay(1, True, 1, straight)
 
         def collect_step(s, _):
             collect(s)
@@ -1289,10 +1305,17 @@
         for t, (to_sp, to_tp, cond) in enumerate(halo_to):
             gathered.start(remote(tail, head, halo_s.at[t], halo_r.at[next_seg], to_sp, to_tp), cond)
         for j in range(ROW_CHUNKS):
+            if j == 1:
+                relay(0, False, 2, crossed)
+                relay(0, True, 2, crossed)
+                relay(1, False, 1, crossed)
+                relay(1, True, 1, crossed)
             if j == ROW_CHUNKS // 2:
                 relay(0, False, 3)
                 relay(1, False, 2, z > 0)
                 relay(1, True, 2, z < nz - 1)
+                crossed_own(4)
+                crossed_own(5)
             if j == ROW_CHUNKS - 1:
                 relay(0, True, 3)
             got = chunk_of(y, 1 - x, j)
@@ -1303,19 +1326,13 @@
             arrived(got, ag_s.at[j, 0], gather_sem(j, 1 - y, x))
             if j % 2 == 1:
                 gathered.start(remote(got, got, ag_s.at[j, 2], gather_sem(j, 1 - y, x), sp, by_x))
-        for p in (4, 5):
-            own_z(p, False)
-            own_z(p, True)
-            own_c(p)
-            crossed_own(p)
-        for j in range(ROW_CHUNKS):
-            arrived(chunk_of(1 - y, 1 - x, j), ag_s.at[j, 0], gather_sem(j, 1 - y, 1 - x))
-        relay(1, False, 2, z == 0)
-        relay(1, True, 2, z == nz - 1)
         for d in range(4, nz):
             relay(0, False, d)
             relay(0, True, d)
-        lax.fori_loop(0, n_sp, release, 0)
+        pl.when(straight)(weight_loads[0].wait)
+        side_arrivals(0)
+        for g, (_, _, cond) in enumerate(halo_from):
+            arrived(rows.at[pl.ds(g * seg, HALO)], halo_s.at[0], halo_r.at[g], cond)
 
         def up_tile(m, start, count):
             r = pl.ds(start, count)
@@ -1325,26 +1342,28 @@
                 total = term if total is None else total + term
             ups[m, r, :] = total.astype(BF16)
 
-        def up_rows(m):
-            def one(i, _):
-                up_tile(m, pl.multiple_of(i * seg, 16), seg)
-                return 0
-
-            lax.fori_loop(0, n_tp, one, 0)
-
-        pl.when(straight)(weight_loads[0].wait)
-        side_arrivals(0)
-        for g, (_, _, cond) in enumerate(halo_from):
-            arrived(rows.at[pl.ds(g * seg, HALO)], halo_s.at[0], halo_r.at[g], cond)
-        up_rows(0)
+        def gate_step(i, _):
+            yy = jnp.where(i >= 2, 1 - y, y)
+            xx = jnp.where(i % 2 == 1, 1 - x, x)
+            up_tile(0, pl.multiple_of((yy * lines + xx) * seg, 16), seg)
+            return 0
+
+        lax.fori_loop(0, n_tp - 1, gate_step, 0)
+        relay(2, False, 1, jnp.logical_and(middle, straight))
+        for j in range(ROW_CHUNKS):
+            arrived(chunk_of(1 - y, 1 - x, j), ag_s.at[j, 0], gather_sem(j, 1 - y, 1 - x))
+        relay(1, False, 2, z == 0)
+        relay(1, True, 2, z == nz - 1)
+        lax.fori_loop(0, n_sp, release, 0)
+
+        lax.fori_loop(n_tp - 1, n_tp, gate_step, 0)
         for d in range(3, nz):
             relay(1, False, d)
             relay(1, True, d)
-        relay(2, False, 1, middle)
+        relay(2, False, 1, jnp.logical_and(middle, crossed))
         relay(2, True, 1, middle)
         pl.when(straight)(weight_loads[1].wait)
         side_arrivals(1)
-        up_rows(1)
 
         arrived(tapb, tap_s.at[0], tap_r.at[0], crossed)
         arrived(shiftb, tap_s.at[1], tap_r.at[1], crossed)
@@ -1362,13 +1381,6 @@
                 jax.nn.gelu(convs[0]) * convs[1]
             ).astype(BF16)
 
-        def activate_step(i, _):
-            for t in range(hidden // hcols):
-                activate(i, pl.ds(t * hcols, hcols))
-            return 0
-
-        lax.fori_loop(0, n_tp, activate_step, 0)
-
         order = [
             [zz] + sorted((o for o in range(nz) if o != zz), key=lambda o: (abs(o - zz), abs(2 * o - nz + 1)))
             for zz in range(nz)
@@ -1386,21 +1398,20 @@
         def seg_rows(yy, xx):
             return pl.ds(pl.multiple_of((yy * lines + xx) * own, own), own)
 
+        def over_x(s, yy):
+            return remote(
+                part.at[s, seg_rows(yy, 1 - x), left], r1.at[s, 0, yy, :, left],
+                f1_s.at[s, yy], f1_r.at[s, yy], sp, by_x,
+            )
+
+        def over_y(s, xx):
+            return remote(
+                part.at[s, seg_rows(1 - y, xx), right], r1.at[s, 0, xx, :, right],
+                f1_s.at[s, ny + xx], f1_r.at[s, ny + xx], by_y, tp,
+            )
+
         def first_hops(s):
-            copies = [
-                remote(
-                    part.at[s, seg_rows(yy, 1 - x), left], r1.at[s, 0, yy, :, left],
-                    f1_s.at[s, yy], f1_r.at[s, yy], sp, by_x,
-                )
-                for yy in range(ny)
-            ]
-            return copies + [
-                remote(
-                    part.at[s, seg_rows(1 - y, xx), right], r1.at[s, 0, xx, :, right],
-                    f1_s.at[s, ny + xx], f1_r.at[s, ny + xx], by_y, tp,
-                )
-                for xx in range(lines)
-            ]
+            return [over_x(s, yy) for yy in range(ny)] + [over_y(s, xx) for xx in range(lines)]
 
         def second_hops(s):
             return [
@@ -1452,31 +1463,46 @@
             return 0
 
         pl.when(straight)(weight_loads[2].wait)
+        for p in (4, 5):
+            arrived(slot(p, z * ny + 1 - c), bulk_z.at[p, 0], bulk_r.at[p, z * ny + 1 - c])
+        early = [me, z * ny + 1 - c]
+
+        def value_step(i, _):
+            to_y, to_x = i % 2 == 0, i < 2
+            yy = jnp.where(to_y, 1 - y, y)
+            xx = jnp.where(to_x, 1 - x, x)
+            g = yy * lines + xx
+            up_tile(1, pl.multiple_of(g * seg, 16), seg)
+            for t in range(hidden // hcols):
+                activate(g, pl.ds(t * hcols, hcols))
+            r = seg_rows(yy, xx)
+            for s in early:
+                part[s, r, :] = dot(act[r, :], wd[s]).astype(BF16)
+                pl.when(to_x)(over_x(s, yy).start)
+                pl.when(to_y)(over_y(s, xx).start)
+            return 0
+
+        lax.fori_loop(0, n_tp, value_step, 0)
+        for d in range(2, nz - 1):
+            relay(2, False, d, middle)
+            relay(2, True, d, middle)
+        for s in early:
+            down_combine(s)
         previous = None
-        done = []
-        for k in range(nz):
+        done = list(early)
+        for k in range(1, nz):
             src_z = nearest(k)
-            if k > 0:
-                src = src_z * ny + c
-                to_z = jnp.where(src_z < z, z + 1, z - 1)
-                more = jnp.logical_and(to_z >= 0, to_z < nz)
-                fresh = jnp.logical_not(jnp.logical_and(middle, jnp.abs(src_z - z) == 1))
-                for p in (4, 5):
-                    arrived(slot(p, src), bulk_z.at[p, 0], bulk_r.at[p, src], fresh)
-                    bulk.start(
-                        remote(
-                            slot(p, src), slot(p, src), bulk_z.at[p, 2 * nz + 2 + k],
-                            bulk_r.at[p, src], to_z * ny + y, tp,
-                        ),
-                        jnp.logical_and(more, fresh),
-                    )
-                    bulk.start(
-                        remote(
-                            slot(p, src), slot(p, src), bulk_c.at[p, 2 * nz + k],
-                            bulk_r.at[p, src], sp, by_c,
-                        ),
-                        fresh,
-                    )
+            src = src_z * ny + c
+            fresh = jnp.logical_not(middle)
+            for p in (4, 5):
+                arrived(slot(p, src), bulk_z.at[p, 0], bulk_r.at[p, src], fresh)
+                bulk.start(
+                    remote(
+                        slot(p, src), slot(p, src), bulk_c.at[p, src_z],
+                        bulk_r.at[p, src], sp, by_c,
+                    ),
+                    fresh,
+                )
             for d in range(cores):
                 src = src_z * ny + (c + d) % cores
                 if d > 0:
@@ -1535,9 +1561,9 @@
         vmem((tok_rows, hidden), BF16),
         dma((9,)),
         dma((6, n_sp)),
-        dma((6, 3 * nz + 2)),
+        dma((6, nz + 1)),
         dma((6,)),
-        dma((6, 3 * nz)),
+        dma((6, nz)),
         dma((2,)),
         dma((2,)),
         dma((oy, heads)),
@@ -1548,10 +1574,6 @@
         dma((heads,)),
         dma((oy, heads)),
         dma((ny, heads)),
-        dma((n_sp, oc, lines)),
-        dma((n_sp, oc, lines)),
-        dma((n_sp, ol)),
-        dma((n_sp, ol)),
         dma((ROW_CHUNKS, 3)),
         dma((ROW_CHUNKS, n_tp)),
         dma((n_tp,)),

time: 189 us -> 180 us (0.952)
  Pallas kernels: 183 us -> 173 us
    pallas_call x1, Pallas kernels: 183 us -> 173 us  [shards(): call(*tables, logs, norm_gain, norm_bias, conv_weight, conv_bias, query_p...]
where the time goes in v3:
time: 180 us; the launch traced here: 178 us
  Pallas kernels  173 us (96%)
  local copies, waits for them, and re-layouts  4.99 us (3%)
    pallas_call x1, Pallas kernels, shards(): call(*tables, logs, norm_gain, norm_bias, conv_weight, conv_bias, query_p...  173 us
    unnamed x2, local copies, waits for them, and re-layouts  3.69 us

profile of v3, /device:TPU:30, one launch (start us, length us, event | category | flops | bytes accessed | tf_op | source)
XLA Modules:
  0.0 177.9 jit_solution(16773045150409627357)
XLA Ops:
  0.0 1.3 reshape.3.log_ref
  1.3 1.4 copy.19.taps
  2.7 172.9 %shard_map.172 = bf16[256,2048]{1,0:T(8,128)(2,1)} custom-call(f32[256,128]{1,0:T(8,128)} %constant.8.clone.cos_in, f32[256,128]{1,0:T(8,128)} %constant.9.clone.sin_in, f32[32,128]{1,0:T(8,128)} %constant.10.clone.cos_out, f32[32,128]{1,0:T(8,128)} %constant.11.clone.sin_out, f32[8,256]{1,0:T(8,128)} %reshape.3.log_ref, f32[2,2048]{1,0:T(2,128)} %gain.1, ...), custom_call_target="tpu_custom_call" | custom-call | tf_op jit(solution)/shard_map/pallas_call | solution.py:1616
  175.6 2.3 %copy.21 = bf16[256,2048]{1,0:T(8,128)(2,1)} copy(bf16[256,2048]{1,0:T(8,128)(2,1)} %shard_map.172) | data formatting | bytes 2097152
